TPU v7x, 128 devices: a whole 4x4x4 slice. The times are simulated.
128 devices in a mesh: sp: 32 (over z, y, core), tp: 4 (over x).
Axes of the slice: x: 4, y: 4, z: 4, core: 2. Of those that a mesh axis runs over, the one named last changes fastest.
Arguments:
- layer_input: bfloat16 [16384, 2048], P('sp'), may hold values from -6 to 6
- out_cot: bfloat16 [16384, 2048], P('sp'), may hold values from -6 to 6
- expert_ids: int32 [16384, 2], P('sp'), may hold values from 0 to 31, all different within a row; in each aligned block of 512 rows (0 to 511, 512 to 1023, ...) at most 40 rows name the same one
- route_weight: float32 [16384, 2], P('sp'), may hold values from 0.1 to 1
- w_gate: bfloat16 [32, 2048, 1024], P('sp', None, 'tp'), may hold values from -0.125 to 0.125
- w_up: bfloat16 [32, 2048, 1024], P('sp', None, 'tp'), may hold values from -0.125 to 0.125
- w_down: bfloat16 [32, 1024, 2048], P('sp', 'tp'), may hold values from -0.1875 to 0.1875
- out_proj: bfloat16 [2048, 1024], P(None, 'tp'), may hold values from -0.1875 to 0.1875
- rec_input: bfloat16 [16384, 1024], P('sp', 'tp'), may hold values from -6 to 6
- gate_input: bfloat16 [16384, 1024], P('sp', 'tp'), may hold values from -6 to 6
- prev_state: float32 [16384, 1024], P('sp', 'tp'), may hold values from -6 to 6
- decay_param: float32 [1024], replicated, may hold values from 4 to 20
- extra_decay: float32 [8, 16384], P('tp', 'sp'), may hold values from -3 to 0, as said below
- gate_a_w: bfloat16 [8, 128, 128], replicated, may hold values from -0.5 to 0.5
- gate_i_w: bfloat16 [8, 128, 128], replicated, may hold values from -0.5 to 0.5
Outputs:
- grad_gate: float32 [32, 2048, 1024], P('sp', None, 'tp')
- grad_up: float32 [32, 2048, 1024], P('sp', None, 'tp')
- grad_down: float32 [32, 1024, 2048], P('sp', 'tp')
- grad_out_proj: float32 [2048, 1024], P('sp', 'tp')
- rec_input_grad: bfloat16 [16384, 1024], P('sp', 'tp')
- gate_input_grad: bfloat16 [16384, 1024], P('sp', 'tp')
Inputs may be any that keep to these rules, and one draw needn't show every extreme that they name: `expert_ids`: each row names 2 different experts; among the slots of the tokens of one sp index (aligned blocks of 512 rows) no expert is named more than 40 times, and in every draw some expert is named exactly 40 times in some block. `extra_decay`: every entry is at most -0.05 / 16384.
All inputs are finite; a program needn't handle non-finite values.
Results may differ from a plain program's by a relative error of at most 0.017.
Values may be sent and summed in bfloat16 or wider, within the bound.
No kernel may reach another device: no remote copies, remote signals or barrier semaphores. Data moves between devices by JAX's collectives and lax.ppermute only.
A program may use at most 128 MiB of HBM per device.

v0:
```python
import functools
import jax
import jax.numpy as jnp
from jax import lax
from jax.experimental import pallas as pl
from jax.experimental.pallas import tpu as pltpu
from jax.sharding import Mesh, PartitionSpec as P


F32 = jnp.float32
BF16 = jnp.bfloat16
gelu_scale = 0.7978845608028654
gelu_cubic = 0.044715
decay_factor = 8.0
ring_steps = (0, 3, 1, 2)


def params(limit_mib=48, **extra):
    return pltpu.CompilerParams(vmem_limit_bytes=limit_mib * 1024 * 1024, **extra)


def cost(flops, moved):
    return pl.CostEstimate(flops=flops, bytes_accessed=moved, transcendentals=0)


def whole(shape):
    return pl.BlockSpec(shape, lambda *_: (0,) * len(shape), pipeline_mode=pl.Buffered(1))


SMEM = pl.BlockSpec(memory_space=pltpu.SMEM)


def made(shape, dtype):
    return pltpu.HBM(shape, dtype)


def kept(arrays):
    return [pltpu.with_memory_space_constraint(a, pltpu.HBM) for a in arrays]


def dot(a, b, dims=((1,), (0,))):
    return lax.dot_general(a, b, (dims, ((), ())), preferred_element_type=F32)


def sigmoid(v):
    return 1.0 / (1.0 + jnp.exp(-v))


def minus_expm1(v):
    series = 1.0 + v / 8.0
    for order in range(7, 1, -1):
        series = 1.0 + v / order * series
    return jnp.where(v > -0.5, -v * series, 1.0 - jnp.exp(v))


def early_kernel(
    where_ref, ids, rec, gate_in, prev, rates, extra, map_a, map_i,
    out_rec, out_act, out_b, out_ca, out_ci, out_cs, out_decay, out_seg, out_exp, out_block, out_sel,
    *, capacity, experts,
):
    tokens, channels = rec.shape
    heads = channels // 128
    first = where_ref[0] * heads

    def block_of_tokens(i, _):
        rows = pl.ds(pl.multiple_of(i * 128, 128), 128)
        for h in range(heads):
            cols = slice(h * 128, (h + 1) * 128)
            values_bf = rec[rows, cols]
            x = values_bf.astype(F32)
            ra = sigmoid(dot(values_bf, map_a[first + h]))
            ig = sigmoid(dot(values_bf, map_i[first + h]))
            rate = rates[pl.ds(first + h, 1), :]
            log_decay = -rate * ra + extra[rows, h : h + 1]
            decay = jnp.exp(log_decay)
            scale = jnp.sqrt(minus_expm1(2.0 * log_decay))
            before = prev[rows, cols]
            state = decay * before + scale * ig * x
            g = gate_in[rows, cols].astype(F32)
            bend = jnp.tanh(gelu_scale * (g + gelu_cubic * g * g * g))
            act = 0.5 * g * (1.0 + bend)
            slope = 0.5 * (1.0 + bend) + 0.5 * g * (1.0 - bend * bend) * gelu_scale * (
                1.0 + 3.0 * gelu_cubic * g * g
            )
            out_rec[rows, cols] = (state * act).astype(BF16)
            out_act[rows, cols] = act
            out_b[rows, cols] = state * slope
            out_ca[rows, cols] = (decay * before - decay * decay / scale * ig * x) * -rate * ra * (1.0 - ra)
            out_ci[rows, cols] = scale * x * ig * (1.0 - ig)
            out_cs[rows, cols] = scale * ig
            out_decay[h, rows, :] = decay
        return 0

    lax.fori_loop(0, tokens // 128, block_of_tokens, 0)
    length = tokens // 8
    for h in range(heads):
        cols = slice(h * 128, (h + 1) * 128)
        product = jnp.ones((8, 128), F32)
        for i in range(length - 1, -1, -1):
            out_seg[h, pl.ds(i, 8, stride=length), :] = product
            product = product * out_decay[h, pl.ds(i, 8, stride=length), :]
        carry = jnp.ones((1, 128), F32)
        for k in range(7, -1, -1):
            rows = slice(k * length, (k + 1) * length)
            out_exp[rows, cols] = out_seg[h, rows, :] * carry
            carry = carry * product[k : k + 1, :]
        out_block[:, cols] = jnp.broadcast_to(carry, (8, 128))
    lane = lax.broadcasted_iota(jnp.int32, (tokens, 128), 1)
    first_id = ids[:, 0:1]
    second_id = ids[:, 1:2]
    one = (lane == first_id).astype(F32)
    two = (lane == second_id).astype(F32)
    lower = lax.broadcasted_iota(jnp.int32, (tokens, tokens), 0) > lax.broadcasted_iota(
        jnp.int32, (tokens, tokens), 1
    )
    rank = dot(lower.astype(F32).astype(BF16), (one + two).astype(BF16))
    place_one = first_id * capacity + jnp.sum(rank * one, axis=1, keepdims=True).astype(jnp.int32)
    place_two = second_id * capacity + jnp.sum(rank * two, axis=1, keepdims=True).astype(jnp.int32)
    slots = experts * capacity

    def block_of_slots(i, _):
        at = pl.multiple_of(i * 256, 256)
        slot = lax.broadcasted_iota(jnp.int32, (tokens, 256), 1) + at
        hit = (slot == place_one) | (slot == place_two)
        out_sel[:, pl.ds(at, 256)] = jnp.where(hit, 1.0, 0.0).astype(BF16)
        return 0

    lax.fori_loop(0, slots // 256, block_of_slots, 0)


def early(position, ids, rec, gate_in, prev, rates, extra, map_a, map_i, capacity, experts):
    tokens, channels = rec.shape
    wide = made((tokens, channels), F32)
    heads = made((channels // 128, tokens, 128), F32)
    outs = (
        made((tokens, channels), BF16),
        wide, wide, wide, wide, wide, heads, heads, wide,
        made((8, channels), F32),
        made((tokens, experts * capacity), BF16),
    )
    args = (position, ids, rec, gate_in, prev, rates, extra, map_a, map_i)
    return pl.pallas_call(
        functools.partial(early_kernel, capacity=capacity, experts=experts),
        out_shape=outs,
        in_specs=[SMEM] + [whole(a.shape) for a in args[1:]],
        out_specs=[whole(o.shape) for o in outs],
        compiler_params=params(14),
        cost_estimate=cost(3 * 10**9, 8 * 2**20),
        name="early",
    )(args[0], *kept(args[1:]))


def build_kernel(where_ref, ids, weight, *refs, capacity, group, weighted):
    sources, out, rank_ref, weight_ref = refs[:-3], refs[-3], refs[-2], refs[-1]
    experts, tokens = rank_ref.shape

    @pl.when(pl.program_id(0) == 0)
    def _():
        name = lax.broadcasted_iota(jnp.int32, (experts, tokens), 0)
        one = jnp.where(name == ids[0:1, :], 1.0, 0.0)
        two = jnp.where(name == ids[1:2, :], 1.0, 0.0)
        both = one + two
        upper = lax.broadcasted_iota(jnp.int32, (tokens, tokens), 0) < lax.broadcasted_iota(
            jnp.int32, (tokens, tokens), 1
        )
        rank = dot(both.astype(BF16), upper.astype(F32).astype(BF16))
        rank_ref[...] = jnp.where(both > 0.0, rank, -1.0)
        weight_ref[...] = one * weight[0:1, :] + two * weight[1:2, :]

    first = pl.program_id(0) * group
    place = lax.broadcasted_iota(jnp.int32, (capacity, tokens), 0).astype(F32)
    picks, weights = [], []
    for e in range(group):
        hit = place == rank_ref[pl.ds(first + e, 1), :]
        picks.append(jnp.where(hit, 1.0, 0.0))
        weights.append(
            jnp.sum(jnp.where(hit, weight_ref[pl.ds(first + e, 1), :], 0.0), axis=1, keepdims=True)
        )
    pick = jnp.concatenate(picks, axis=0).astype(BF16)
    by = jnp.concatenate(weights, axis=0)
    at = 0
    for source, scaled in zip(sources, weighted):
        rows = dot(pick, source[...])
        if scaled:
            rows = rows * by
        out[:, at : at + source.shape[1]] = rows.astype(BF16)
        at += source.shape[1]


def build(position, ids, weight, parts, capacity, experts, group=8):
    tokens = ids.shape[1]
    total = sum(width for _, width, _, _ in parts)
    specs = [pl.BlockSpec(ids.shape, lambda i, where: (0, 0))] * 2
    for _, width, column, _ in parts:
        specs.append(pl.BlockSpec((tokens, width), functools.partial(column_block, column)))
    return pl.pallas_call(
        functools.partial(
            build_kernel, capacity=capacity, group=group, weighted=tuple(p[3] for p in parts)
        ),
        out_shape=made((experts * capacity, total), BF16),
        grid_spec=pltpu.PrefetchScalarGridSpec(
            num_scalar_prefetch=1,
            grid=(experts // group,),
            in_specs=specs,
            out_specs=pl.BlockSpec((group * capacity, total), lambda i, where: (i, 0)),
            scratch_shapes=[pltpu.VMEM((experts, tokens), F32), pltpu.VMEM((experts, tokens), F32)],
        ),
        compiler_params=params(14),
        cost_estimate=cost(1400000 * total, 5000 * total),
    )(position, *kept([ids, weight, *(p[0] for p in parts)]))


def column_block(column, i, where):
    return (0, where[0] if column is None else column)


def weights_kernel(
    where_ref, w_gate, w_up, w_down, whole_own, *refs, row_part, cot_part,
):
    pieces = refs[:8]
    out_gate_up, out_down, out_gate, out_up = refs[8:]
    at, core = where_ref[0], where_ref[1]
    width, units = w_gate.shape
    half = width // 2
    first = ((0,), (0,))
    mine = pl.multiple_of(core * half, half)
    other = pl.multiple_of(half - core * half, half)
    for weights, out in ((w_gate, out_gate), (w_up, out_up)):
        out[at] = dot(weights[...], whole_own[...], first).astype(BF16)
        for step, n in ((3, 0), (1, 1)):
            out[lax.rem(at + step, 4)] = (
                dot(weights[pl.ds(mine, half), :], pieces[n][...], first)
                + dot(weights[pl.ds(other, half), :], pieces[4 + n][...], first)
            ).astype(BF16)
        quarter = half // 2
        out[lax.rem(at + 2, 4)] = sum(
            dot(weights[pl.ds(start + n * quarter, quarter), :], pieces[side + 2 + n][...], first)
            for start, side in ((mine, 0), (other, 4))
            for n in range(2)
        ).astype(BF16)
    rest = width - 4 * row_part
    out_gate_up[:rest, :units] = w_gate[4 * row_part :, :]
    out_gate_up[:rest, units:] = w_up[4 * row_part :, :]
    cot_rest = width - 4 * cot_part
    out_down[:cot_rest, :] = w_down[:, 4 * cot_part :].T
    for n, step in enumerate((2, 0, 3, 1)):
        group = lax.rem(at + step, 4)
        lines = pl.ds(pl.multiple_of(group * row_part, row_part), row_part)
        columns = pl.ds(pl.multiple_of(group * cot_part, 128), cot_part)
        to = slice(rest + n * row_part, rest + (n + 1) * row_part)
        out_gate_up[to, :units] = w_gate[lines, :]
        out_gate_up[to, units:] = w_up[lines, :]
        to = slice(cot_rest + n * cot_part, cot_rest + (n + 1) * cot_part)
        out_down[to, :] = w_down[:, columns].T


def folded_weights(position, w_gate, w_up, w_down, own, pieces, row_part, cot_part):
    width, units = w_gate.shape
    args = (position, w_gate, w_up, w_down, own, *pieces)
    fold = made((4, units, own.shape[1]), BF16)
    outs = (made((width, 2 * units), BF16), made((width, units), BF16), fold, fold)
    return pl.pallas_call(
        functools.partial(weights_kernel, row_part=row_part, cot_part=cot_part),
        out_shape=outs,
        in_specs=[SMEM] + [whole(a.shape) for a in args[1:]],
        out_specs=[whole(o.shape) for o in outs],
        compiler_params=params(24),
        cost_estimate=cost(4 * 10**9, 7 * 2**20),
        name="folded",
    )(position, *kept([w_gate, w_up, w_down, own]), *pieces)


def ahead_kernel(gate_up, down, *refs, row_part, row_from, cot_from):
    pieces, out = refs[:-1], refs[-1]
    half = pieces[0].shape[0]
    wide = gate_up.shape[1]
    for n in range(2):
        lines = slice(n * half, (n + 1) * half)
        rows = jnp.concatenate([p[:, :row_part] for p in pieces[n::2]], axis=1)
        cots = jnp.concatenate([p[:, row_part:] for p in pieces[n::2]], axis=1)
        out[lines, :wide] = dot(rows, gate_up[row_from:, :])
        out[lines, wide:] = dot(cots, down[cot_from:, :])


def ahead(pieces, gate_up, down, row_part, cot_part):
    width = gate_up.shape[0]
    out = made((2 * pieces[0].shape[0], gate_up.shape[1] + down.shape[1]), F32)
    args = (gate_up, down, *pieces)
    return pl.pallas_call(
        functools.partial(
            ahead_kernel,
            row_part=row_part,
            row_from=width - 3 * row_part,
            cot_from=width - 3 * cot_part,
        ),
        out_shape=out,
        in_specs=[whole(a.shape) for a in args],
        out_specs=whole(out.shape),
        compiler_params=params(20),
        cost_estimate=cost(2 * 10**9, 12 * 2**20),
        name="ahead",
    )(*kept([gate_up, down]), *pieces)


def expert_kernel(
    got_rows, got_cot, far_top, far_bottom, before, gate_up, down, fold_gate, fold_up,
    out_hidden, out_gate, out_up, out_mix, *, row_part,
):
    units = down.shape[1]
    upper = pl.program_id(0) < pl.num_programs(0) // 2
    far = jnp.where(upper, far_top[...], far_bottom[...])
    rows = jnp.concatenate([got_rows[...], far[:, :row_part]], axis=1)
    cots = jnp.concatenate([got_cot[...], far[:, row_part:]], axis=1)
    both = dot(rows, gate_up[...]) + before[:, : 2 * units]
    gate_pre, up_pre = both[:, :units], both[:, units:]
    hidden_cot = dot(cots, down[...]) + before[:, 2 * units :]
    sigma = sigmoid(gate_pre)
    swish = gate_pre * sigma
    out_hidden[...] = (swish * up_pre).astype(BF16)
    gate_cot = (hidden_cot * up_pre * sigma * (1.0 + gate_pre * (1.0 - sigma))).astype(BF16)
    up_cot = (hidden_cot * swish).astype(BF16)
    out_gate[...] = gate_cot
    out_up[...] = up_cot
    for c in range(4):
        out_mix[c] = (dot(gate_cot, fold_gate[c]) + dot(up_cot, fold_up[c])).astype(BF16)


def first_rows(array, count):
    return pl.BlockSpec(
        (count, array.shape[1]), lambda i: (0, 0), pipeline_mode=pl.Buffered(1)
    )


def expert(got, far, before, gate_up, down, fold_gate, fold_up, row_part, cot_part, steps=4):
    rows = got.shape[0]
    width, hidden = down.shape
    block = rows // steps
    part = fold_gate.shape[2]
    half = steps // 2
    row_rest, cot_rest = width - 4 * row_part, width - 4 * cot_part
    narrow = made((rows, hidden), BF16)
    mine = pl.BlockSpec((block, hidden), lambda i: (i, 0))
    return pl.pallas_call(
        functools.partial(expert_kernel, row_part=row_part),
        out_shape=(narrow, narrow, narrow, made((4, rows, part), BF16)),
        grid=(steps,),
        in_specs=[
            pl.BlockSpec((block, row_rest), lambda i: (i, 0)),
            pl.BlockSpec((block, cot_rest), lambda i: (i, row_rest // cot_rest)),
            pl.BlockSpec((block, row_part + cot_part), lambda i: (jnp.minimum(i, half - 1), 0)),
            pl.BlockSpec((block, row_part + cot_part), lambda i: (jnp.maximum(i - half, 0), 0)),
            pl.BlockSpec((block, before.shape[1]), lambda i: (i, 0)),
            first_rows(gate_up, row_rest + row_part),
            first_rows(down, cot_rest + cot_part),
            whole(fold_gate.shape),
            whole(fold_up.shape),
        ],
        out_specs=[mine, mine, mine, pl.BlockSpec((4, block, part), lambda i: (0, i, 0))],
        compiler_params=params(26),
        cost_estimate=cost(5 * 10**9, 16 * 2**20),
        name="expert",
    )(*kept([got, got]), *far, *kept([before, gate_up, down, fold_gate, fold_up]))


def row_grads_kernel(where_ref, got_rows, *refs, row_part):
    pieces = refs[:8]
    gate_cot, up_cot, out_gate, out_up = refs[8:]
    at = where_ref[0]
    first = ((0,), (0,))
    rows = got_rows[...]
    out_gate[0, 4 * row_part :, :] = dot(rows, gate_cot[...], first)
    out_up[0, 4 * row_part :, :] = dot(rows, up_cot[...], first)
    for n, step in enumerate(ring_steps):
        group = lax.rem(at + step, 4)
        top, bottom = pieces[2 * n], pieces[2 * n + 1]
        half = top.shape[0]
        lines = pl.ds(pl.multiple_of(group * row_part, row_part), row_part)
        for cot, out in ((gate_cot, out_gate), (up_cot, out_up)):
            out[0, lines, :] = dot(top[...], cot[:half, :], first) + dot(
                bottom[...], cot[half:, :], first
            )


def down_grads_kernel(where_ref, got_cot, *refs, row_part, cot_part):
    pieces = refs[:8]
    hidden, out_down = refs[8:]
    at = where_ref[0]
    first = ((0,), (0,))
    out_down[0, :, 4 * cot_part :] = dot(hidden[...], got_cot[...], first)
    for n, step in enumerate(ring_steps):
        group = lax.rem(at + step, 4)
        top, bottom = pieces[2 * n], pieces[2 * n + 1]
        half = top.shape[0]
        columns = pl.ds(pl.multiple_of(group * cot_part, 128), cot_part)
        out_down[0, :, columns] = dot(hidden[:half, :], top[:, row_part:], first) + dot(
            hidden[half:, :], bottom[:, row_part:], first
        )


def columns_of(array, width, index):
    return pl.BlockSpec(
        (array.shape[0], width), lambda i: (0, index), pipeline_mode=pl.Buffered(1)
    )


def row_grads(position, got, pieces, gate_cot, up_cot, width, row_part):
    row_rest = width - 4 * row_part
    out = made((1, width, gate_cot.shape[1]), F32)
    return pl.pallas_call(
        functools.partial(row_grads_kernel, row_part=row_part),
        out_shape=(out, out),
        grid=(1,),
        in_specs=[
            SMEM,
            columns_of(got, row_rest, 0),
            *(columns_of(p, row_part, 0) for p in pieces),
            whole(gate_cot.shape),
            whole(up_cot.shape),
        ],
        out_specs=[whole(out.shape)] * 2,
        compiler_params=params(22),
        cost_estimate=cost(3 * 10**9, 11 * 2**20),
        name="rowgrads",
    )(position, *kept([got, *pieces, gate_cot, up_cot]))


def down_grads(position, got, pieces, hidden, width, row_part, cot_part):
    row_rest, cot_rest = width - 4 * row_part, width - 4 * cot_part
    out = made((1, hidden.shape[1], width), F32)
    return pl.pallas_call(
        functools.partial(down_grads_kernel, row_part=row_part, cot_part=cot_part),
        out_shape=out,
        grid=(1,),
        in_specs=[
            SMEM,
            columns_of(got, cot_rest, row_rest // cot_rest),
            *(whole(p.shape) for p in pieces),
            whole(hidden.shape),
        ],
        out_specs=whole(out.shape),
        compiler_params=params(20),
        cost_estimate=cost(15 * 10**8, 11 * 2**20),
        name="downgrads",
    )(position, *kept([got, *pieces, hidden]))


def proj_kernel(where_ref, gate_cot, up_cot, w_gate, w_up, local, *refs):
    pieces, out = refs[:-1], refs[-1]
    core = where_ref[1]
    first = ((0,), (0,))
    for n, step in enumerate(ring_steps):
        top, bottom = pieces[2 * n], pieces[2 * n + 1]
        half = top.shape[0]
        push_gate, push_up = (
            (dot(cot[:half, :], top[...], first) + dot(cot[half:, :], bottom[...], first)).astype(BF16)
            for cot in (gate_cot, up_cot)
        )
        term = dot(w_gate[...], push_gate) + dot(w_up[...], push_up)
        if step == 0:
            term = term + local[...]
        term = term.astype(BF16)
        lines = out.shape[3]
        for s in range(2 * out.shape[2]):
            slot = lax.rem(s % 2 + core, 2)
            out[slot, n, s // 2] = term[s * lines : (s + 1) * lines, :]


def proj(position, gate_cot, up_cot, w_gate, w_up, local, pieces, lines):
    width, part = w_gate.shape[0], pieces[0].shape[1]
    args = (position, gate_cot, up_cot, w_gate, w_up, local, *pieces)
    out = made((2, 4, width // lines // 2, lines, part), BF16)
    return pl.pallas_call(
        proj_kernel,
        out_shape=out,
        in_specs=[SMEM] + [whole(a.shape) for a in args[1:]],
        out_specs=whole(out.shape),
        compiler_params=params(22),
        cost_estimate=cost(4 * 10**9, 14 * 2**20),
        name="proj",
    )(position, *kept(args[1:6]), *pieces)


def chip_kernel(kept_ref, other, out_own, *outs):
    half = out_own.shape[0] // 2
    out_own[...] = (kept_ref[0, 0].astype(F32) + other[0].astype(F32)).astype(BF16)
    for n in range(6):
        lines = slice((n % 2) * half, (n % 2 + 1) * half)
        at = 1 + n // 2
        outs[n][...] = (
            kept_ref[0, at, lines].astype(F32) + other[at, lines].astype(F32)
        ).astype(BF16)


def chip_sum(parts, other):
    groups, lines, width = other.shape[1:]
    half = made((groups // 2, lines, width), BF16)
    outs = (made((groups, lines, width), BF16),) + (half,) * 6
    return pl.pallas_call(
        chip_kernel,
        out_shape=outs,
        grid=(1,),
        in_specs=[
            pl.BlockSpec(
                (1, *parts.shape[1:]), lambda i: (0, 0, 0, 0, 0), pipeline_mode=pl.Buffered(1)
            ),
            whole(other.shape),
        ],
        out_specs=[whole(o.shape) for o in outs],
        compiler_params=params(16),
        cost_estimate=cost(10**7, 6 * 2**20),
        name="chipsum",
    )(*kept([parts]), other)


def scan_kernel(back, sel, base, act, b, decay, seg, block, out_grad, out_local, out_pair, drive, part):
    tokens, channels = base.shape
    length = tokens // 8
    mix = base[...]
    total = back[0].astype(F32) + back[1].astype(F32) + back[2].astype(F32) + back[3].astype(F32)
    mix = mix + dot(sel[...], total.astype(BF16))
    out_grad[...] = (mix * b[...]).astype(BF16)
    push = mix * act[...]
    for h in range(channels // 128):
        cols = slice(h * 128, (h + 1) * 128)
        drive[h] = push[:, cols]
        value = drive[h, pl.ds(length - 1, 8, stride=length), :]
        part[h, pl.ds(length - 1, 8, stride=length), :] = value
        for i in range(length - 2, -1, -1):
            value = (
                drive[h, pl.ds(i, 8, stride=length), :]
                + decay[h, pl.ds(i + 1, 8, stride=length), :] * value
            )
            part[h, pl.ds(i, 8, stride=length), :] = value
        lead = decay[h, pl.ds(0, 8, stride=length), :]
        inner = seg[h, pl.ds(0, 8, stride=length), :]
        carry = jnp.zeros((1, 128), F32)
        for k in range(7, -1, -1):
            rows = slice(k * length, (k + 1) * length)
            out_local[rows, cols] = part[h, rows, :] + seg[h, rows, :] * carry
            one = slice(k, k + 1)
            carry = lead[one, :] * (value[one, :] + inner[one, :] * carry)
        pair = jnp.concatenate([carry, block[0:1, cols]], axis=0)
        out_pair[:, :, cols] = jnp.broadcast_to(pair[None], (out_pair.shape[0], *pair.shape))


def scanned(back, sel, base, act, b, decay, seg, block, sources):
    tokens, channels = base.shape
    args = (back, sel, base, act, b, decay, seg, block)
    outs = (
        made((tokens, channels), BF16),
        made((tokens, channels), F32),
        made((sources, 2, channels), F32),
    )
    return pl.pallas_call(
        scan_kernel,
        out_shape=outs,
        in_specs=[whole(a.shape) for a in args],
        out_specs=[whole(o.shape) for o in outs],
        scratch_shapes=[pltpu.VMEM(decay.shape, F32), pltpu.VMEM(decay.shape, F32)],
        compiler_params=params(14),
        cost_estimate=cost(4 * 10**8, 8 * 2**20),
        name="scanned",
    )(back, *kept(args[1:]))


def final_kernel(where_ref, pairs, local, exp, ca, ci, cs, map_a, map_i, out):
    channels = local.shape[1]
    heads = channels // 128
    first = where_ref[0] * heads
    total = jnp.zeros((1, channels), F32)
    me = where_ref[2]
    for s in range(pairs.shape[0] - 1, 0, -1):
        total = jnp.where(me < s, pairs[s, 0:1, :] + pairs[s, 1:2, :] * total, total)
    for h in range(heads):
        cols = slice(h * 128, (h + 1) * 128)
        cot = local[:, cols] + exp[:, cols] * total[:, cols]
        a_cot = (cot * ca[:, cols]).astype(BF16)
        i_cot = (cot * ci[:, cols]).astype(BF16)
        result = (
            cot * cs[:, cols]
            + dot(a_cot, map_a[first + h], ((1,), (1,)))
            + dot(i_cot, map_i[first + h], ((1,), (1,)))
        )
        out[:, cols] = result.astype(BF16)


def final(position, pairs, local, exp, ca, ci, cs, map_a, map_i):
    args = (position, pairs, local, exp, ca, ci, cs, map_a, map_i)
    return pl.pallas_call(
        final_kernel,
        out_shape=made(local.shape, BF16),
        in_specs=[SMEM] + [whole(a.shape) for a in args[1:]],
        out_specs=whole(local.shape),
        compiler_params=params(8),
        cost_estimate=cost(10**8, 4 * 2**20),
        name="final",
    )(position, pairs, *kept(args[2:]))


def shifted(piece, by):
    return lax.ppermute(piece, "tp", [(i, (i + by) % 4) for i in range(4)])


def ring_gather(top, bottom):
    left_top, right_bottom = shifted(top, 1), shifted(bottom, -1)
    left_bottom, right_top = shifted(bottom, 1), shifted(top, -1)
    far_top, far_bottom = shifted(left_top, 1), shifted(right_bottom, -1)
    return top, bottom, left_top, left_bottom, right_top, right_bottom, far_top, far_bottom


def shared_ring_gather(own, core):
    half = own.shape[0] // 2
    mine = lax.dynamic_slice_in_dim(own, core * half, half, 0)
    left, right = shifted(mine, 1), shifted(mine, -1)
    quarter = half // 2
    far_top, far_bottom = shifted(left[:quarter], 1), shifted(right[quarter:], -1)
    pieces = (left, right, far_top, far_bottom)
    others = tuple(lax.ppermute(p, "core", [(0, 1), (1, 0)]) for p in pieces)
    return pieces + others


def per_device(
    layer_input, out_cot, expert_ids, route_weight, w_gate, w_up, w_down, out_proj,
    rec_input, gate_input, prev_state, decay_param, extra_decay, gate_a_w, gate_i_w,
):
    sources = lax.axis_size("sq") * lax.axis_size("core")
    tp = lax.axis_index("tp")
    core = lax.axis_index("core")
    sp_axes = ("sq", "core")
    sp = lax.axis_index("sq") * 2 + core
    position = jnp.stack([tp, core, sp]).astype(jnp.int32)
    w_gate, w_up, w_down = w_gate[0], w_up[0], w_down[0]
    tokens, width = layer_input.shape
    capacity = 5 * tokens * expert_ids.shape[1] // (4 * sources)
    slots = sources * capacity
    row_part, cot_part = width // 8, 3 * width // 16
    row_rest, cot_rest = width - 4 * row_part, width - 4 * cot_part
    ids, weight = expert_ids.T, route_weight.T

    def exchanged(rows):
        return lax.all_to_all(
            rows.reshape(sources, capacity, -1), sp_axes, 0, 0, tiled=True
        ).reshape(rows.shape)

    spread = build(
        position, ids, weight,
        [(layer_input, row_part, None, False), (out_cot, cot_part, None, True)],
        capacity, sources,
    )
    spread = exchanged(spread)
    projections = shared_ring_gather(out_proj, core)
    gate_up, down, fold_gate, fold_up = folded_weights(
        position, w_gate, w_up, w_down, out_proj, projections, row_part, cot_part
    )
    rates = (decay_factor * jax.nn.softplus(-decay_param)).reshape(-1, gate_a_w.shape[1])
    rec_output, act, b, ca, ci, cs, decay, seg, exp, block, sel = early(
        position, expert_ids, rec_input, gate_input, prev_state, rates, extra_decay.T,
        gate_a_w, gate_i_w, capacity, sources,
    )
    direct = build(
        position, ids, weight,
        [
            (layer_input, row_rest, 4 * row_part // row_rest, False),
            (out_cot, cot_rest, 4 * cot_part // cot_rest, True),
            (rec_output, rec_output.shape[1], 0, False),
        ],
        capacity, sources,
    )
    got = exchanged(direct)
    pieces = ring_gather(spread[: slots // 2], spread[slots // 2 :])
    base = jnp.dot(out_cot, out_proj, preferred_element_type=F32)
    local_proj = lax.dot_general(
        out_cot, rec_output, (((0,), (0,)), ((), ())), preferred_element_type=F32
    )
    before = ahead(pieces[:6], gate_up, down, row_part, cot_part)
    hidden, gate_cot, up_cot, mix = expert(
        got, pieces[6:], before, gate_up, down, fold_gate, fold_up, row_part, cot_part
    )
    back = lax.all_to_all(
        mix.reshape(4 * sources, capacity, -1), ("tp", *sp_axes), 0, 0, tiled=True
    ).reshape(mix.shape)
    grad_gate, grad_up = row_grads(position, got, pieces, gate_cot, up_cot, width, row_part)
    grad_down = down_grads(position, got, pieces, hidden, width, row_part, cot_part)
    start = row_rest + cot_rest
    recs = ring_gather(got[: slots // 2, start:], got[slots // 2 :, start:])
    lines = width // sources
    parts = proj(position, gate_cot, up_cot, w_gate, w_up, local_proj, recs, lines)
    other = lax.ppermute(parts[1], "core", [(0, 1), (1, 0)])
    own, left_top, left_bottom, right_top, right_bottom, far_top, far_bottom = chip_sum(
        parts, other
    )
    through_top, through_bottom = shifted(far_top, 1), shifted(far_bottom, -1)
    from_left, from_right = shifted(right_bottom, 1), shifted(left_top, -1)
    both_top = (right_top.astype(F32) + through_top.astype(F32)).astype(BF16)
    both_bottom = (left_bottom.astype(F32) + through_bottom.astype(F32)).astype(BF16)
    last_top, last_bottom = shifted(both_top, 1), shifted(both_bottom, -1)
    arriving = (
        jnp.concatenate([last_top, last_bottom], axis=0).astype(F32)
        + jnp.concatenate([from_right, from_left], axis=0).astype(F32)
        + own.astype(F32)
    ).astype(BF16)
    arrived = lax.all_to_all(arriving, "sq", 0, 0, tiled=True)
    grad_out_proj = arrived.astype(F32).sum(axis=0)
    gate_input_grad, local, pair = scanned(
        back, sel, base, act, b, decay, seg, block, sources
    )
    pairs = lax.all_to_all(pair, sp_axes, 0, 0, tiled=True)
    rec_input_grad = final(position, pairs, local, exp, ca, ci, cs, gate_a_w, gate_i_w)
    return (grad_gate, grad_up, grad_down, grad_out_proj, rec_input_grad, gate_input_grad)


def solution(mesh):
    sp, tp = mesh.devices.shape
    inner = Mesh(mesh.devices.reshape(sp // 2, 2, tp), ("sq", "core", "tp"))
    sp = ("sq", "core")
    in_specs = (
        P(sp, None),
        P(sp, None),
        P(sp, None),
        P(sp, None),
        P(sp, None, "tp"),
        P(sp, None, "tp"),
        P(sp, "tp", None),
        P(None, "tp"),
        P(sp, "tp"),
        P(sp, "tp"),
        P(sp, "tp"),
        P(),
        P("tp", sp),
        P(),
        P(),
    )
    out_specs = (
        P(sp, None, "tp"),
        P(sp, None, "tp"),
        P(sp, "tp", None),
        P(sp, "tp"),
        P(sp, "tp"),
        P(sp, "tp"),
    )
    return jax.shard_map(
        per_device, mesh=inner, in_specs=in_specs, out_specs=out_specs, check_vma=False
    )
```

profile of v0, /device:TPU:1, one launch (start us, length us, event | category | flops | bytes accessed | tf_op | source)
XLA Modules:
  0.0 257.2 jit_solution(11590163429967273969)
XLA Ops:
  0.7 4.7 %shard_map.191 = bf16[1280,640]{1,0:T(8,128)(2,1)} custom-call(s32[3]{0:T(128)S(1)} %pad_add_fusion.where_ref, s32[2,512]{1,0:T(2,128)} %bitcast.41, f32[2,512]{1,0:T(2,128)} %bitcast.43, bf16[512,2048]{1,0:T(8,128)(2,1)} %refs_0_.3, bf16[512,2048]{1,0:T(8,128)(2,1)} %refs_1_.3), custom_call_target="tpu_custom_call" | custom-call | flops 896000000 | bytes 3200000 | tf_op jit(solution)/shard_map/pallas_call | solution.py:196
  5.4 9.7 %all-to-all-start.1 = ((bf16[32,40,640]{2,1,0:T(8,128)(2,1)}), bf16[32,40,640]{2,1,0:T(8,128)(2,1)S(1)}, u32[]{:S(2)}, u32[]{:S(2)}) async-start(bf16[32,40,640]{2,1,0:T(8,128)(2,1)} %bitcast.37), calls=%async_computation.1 | async-start | bytes 3276800 | tf_op jit(solution)/shard_map/all_to_all | solution.py:641
  15.2 0.9 copy.22.ids
  16.0 0.9 copy.21
  17.5 8.4 %early.1 = (bf16[512,256]{1,0:T(8,128)(2,1)}, f32[512,256]{1,0:T(8,128)}, f32[512,256]{1,0:T(8,128)}, f32[512,256]{1,0:T(8,128)}, f32[512,256]{1,0:T(8,128)}, /*...) custom-call(s32[3]{0:T(128)S(1)} %pad_add_fusion.where_ref, ...), custom_call_target="tpu_custom_call" | custom-call | flops 3000000000 | bytes 8388608 | tf_op jit(solution)/shard_map/early/pallas_call | solution.py:142
  25.9 6.8 %shard_map.190 = bf16[1280,1792]{1,0:T(8,128)(2,1)} custom-call(s32[3]{0:T(128)S(1)} %pad_add_fusion.where_ref, s32[2,512]{1,0:T(2,128)} %bitcast.42, f32[2,512]{1,0:T(2,128)} %bitcast.44, bf16[512,2048]{1,0:T(8,128)(2,1)} %refs_0_.3, bf16[512,2048]{1,0:T(8,128)(2,1)} %refs_1_.3, bf16[512,256]{1,0:T(8,128)(2,1)} %get-tuple-element.37.refs_2_), custom_call_target="tpu_custom_call" | custom-call | flops 2508800000 | bytes 8960000 | tf_op jit(solution)/shard_map/pallas_call | solution.py:196
  32.7 6.0 %all-to-all-done.1 = bf16[32,40,640]{2,1,0:T(8,128)(2,1)S(1)} async-done(((bf16[32,40,640]{2,1,0:T(8,128)(2,1)}), bf16[32,40,640]{2,1,0:T(8,128)(2,1)S(1)}, u32[]{:S(2)}, u32[]{:S(2)}) %all-to-all-start.1) | async-done | bytes 1638432 | tf_op jit(solution)/shard_map/all_to_all | solution.py:641
  38.8 1.2 copy-done.18
  39.9 5.8 %all-to-all-start = ((bf16[32,40,1792]{2,1,0:T(8,128)(2,1)}), bf16[32,40,1792]{2,1,0:T(8,128)(2,1)}, u32[]{:S(2)}, u32[]{:S(2)}) async-start(bf16[32,40,1792]{2,1,0:T(8,128)(2,1)} %bitcast.38), calls=%async_computation | async-start | bytes 9175040 | tf_op jit(solution)/shard_map/all_to_all | solution.py:641
  45.8 1.3 collective-permute-start.6
  47.1 1.5 collective-permute-start.7
  48.6 1.5 fusion.3
  50.2 2.7 %collective-permute-start.3 = (bf16[640,640]{1,0:T(8,128)(2,1)S(1)}, bf16[640,640]{1,0:T(8,128)(2,1)S(1)}, u32[]{:S(2)}, u32[]{:S(2)}) collective-permute-start(bf16[640,640]{1,0:T(8,128)(2,1)S(1)} %bitcast.26), channel_id=1, source_target_pairs={{0,3},{1,0},{2,1},{3,2},{4,7},{5,4},{6,5},{7,6},{8,11},{9,8},{10,9... | collective-permute-start | bytes 2457608 | tf_op jit(solution)/shard_map/ppermute | solution.py:601
  52.9 7.4 %collective-permute-done.6.refs_0_ = bf16[1024,256]{1,0:T(8,128)(2,1)S(1)} collective-permute-done((bf16[1024,256]{1,0:T(8,128)(2,1)S(1)}, bf16[1024,256]{1,0:T(8,128)(2,1)S(1)}, u32[]{:S(2)}, u32[]{:S(2)}) %collective-permute-start.6) | collective-permute-done | bytes 524320 | tf_op jit(solution)/shard_map/ppermute | solution.py:601
  60.4 1.0 slice.39
  61.3 2.7 %collective-permute-start.9 = (bf16[512,256]{1,0:T(8,128)(2,1)S(1)}, bf16[512,256]{1,0:T(8,128)(2,1)S(1)}, u32[]{:S(2)}, u32[]{:S(2)}) collective-permute-start(bf16[512,256]{1,0:T(8,128)(2,1)S(1)} %slice.39), channel_id=1, source_target_pairs={{0,3},{1,0},{2,1},{3,2},{4,7},{5,4},{6,5},{7,6},{8,11},{9,8},{10,9... | collective-permute-start | bytes 786440 | tf_op jit(solution)/shard_map/ppermute | solution.py:601
  64.1 2.6 %collective-permute-start.10 = (bf16[1024,256]{1,0:T(8,128)(2,1)S(1)}, bf16[1024,256]{1,0:T(8,128)(2,1)S(1)}, u32[]{:S(2)}, u32[]{:S(2)}) collective-permute-start(bf16[1024,256]{1,0:T(8,128)(2,1)S(1)} %collective-permute-done.6.refs_0_), channel_id=1, source_target_pairs={{0,4},{4,0},{1,5},{5,1},{2,6},{6,2},{3,7},{7,3},{8,12},{12,8},{9,1... | collective-permute-start | bytes 1572872 | tf_op jit(solution)/shard_map/ppermute | solution.py:618
  66.7 0.8 copy-done.4
  67.5 16.0 %collective-permute-done.8.refs_2_ = bf16[512,256]{1,0:T(8,128)(2,1)S(1)} collective-permute-done((bf16[512,256]{1,0:T(8,128)(2,1)S(1)}, bf16[512,256]{1,0:T(8,128)(2,1)S(1)}, u32[]{:S(2)}, u32[]{:S(2)}) %collective-permute-start.8) | collective-permute-done | bytes 262176 | tf_op jit(solution)/shard_map/ppermute | solution.py:601
  83.4 1.2 collective-permute-start.12
  86.0 0.7 copy-done.12
  88.2 0.8 copy-done.6
  89.0 2.7 %collective-permute-start.2 = (bf16[640,640]{1,0:T(8,128)(2,1)S(1)}, bf16[640,640]{1,0:T(8,128)(2,1)}, u32[]{:S(2)}, u32[]{:S(2)}) collective-permute-start(bf16[640,640]{1,0:T(8,128)(2,1)S(1)} %bitcast.32), channel_id=1, source_target_pairs={{0,3},{1,0},{2,1},{3,2},{4,7},{5,4},{6,5},{7,6},{8,11},{9,8},{10,9... | collective-permute-start | bytes 2457608 | tf_op jit(solution)/shard_map/ppermute | solution.py:601
  91.7 2.7 %collective-permute-start.5 = (bf16[640,640]{1,0:T(8,128)(2,1)S(1)}, bf16[640,640]{1,0:T(8,128)(2,1)}, u32[]{:S(2)}, u32[]{:S(2)}) collective-permute-start(bf16[640,640]{1,0:T(8,128)(2,1)S(1)} %collective-permute-done.3.refs_5_), channel_id=1, source_target_pairs={{0,3},{1,0},{2,1},{3,2},{4,7},{5,4},{6,5},{7,6},{8,11},{9,8},{10,9... | collective-permute-start | bytes 2457608 | tf_op jit(solution)/shard_map/ppermute | solution.py:601
  94.4 2.3 convolution_bitcast_fusion.local
  96.7 3.8 %all-to-all-done = bf16[32,40,1792]{2,1,0:T(8,128)(2,1)} async-done(((bf16[32,40,1792]{2,1,0:T(8,128)(2,1)}), bf16[32,40,1792]{2,1,0:T(8,128)(2,1)}, u32[]{:S(2)}, u32[]{:S(2)}) %all-to-all-start) | async-done | bytes 4587552 | tf_op jit(solution)/shard_map/all_to_all | solution.py:641
  100.5 1.1 fusion.2
  101.6 1.3 collective-permute-start.14
  102.9 4.5 %collective-permute-done.1.refs_3_ = bf16[640,640]{1,0:T(8,128)(2,1)} collective-permute-done((bf16[640,640]{1,0:T(8,128)(2,1)S(1)}, bf16[640,640]{1,0:T(8,128)(2,1)}, u32[]{:S(2)}, u32[]{:S(2)}) %collective-permute-start.1) | collective-permute-done | bytes 819232 | tf_op jit(solution)/shard_map/ppermute | solution.py:601
  107.4 1.3 collective-permute-start.17
  108.6 1.0 copy-done.5
  109.7 1.0 copy-done.7
  110.7 0.9 copy-done.9
  111.6 0.9 copy-done.11
  112.6 0.9 copy-done.13
  113.6 0.9 copy-done.15
  114.5 7.1 %folded.1 = (bf16[2048,512]{1,0:T(8,128)(2,1)}, bf16[2048,256]{1,0:T(8,128)(2,1)}, bf16[4,256,256]{2,1,0:T(8,128)(2,1)}, bf16[4,256,256]{2,1,0:T(8,128)(2,1)}) custom-call(s32[3]{0:T(128)S(1)} %pad_add_fusion.where_ref, bf16[2048,256]{1,0:T(8,128)(2,1)} %bitcast.46, bf16[2048,256]{1,0:T(8,128)(2,1)} %bitcast.48, bf16[256,2048]{1,0:T(8,128)(2,1)} %bitcast.45, ...), custom_call_target="tpu_custom_call" | custom-call | flops 4000000000 | bytes 7340032 | tf_op jit(solution)/shard_map/folded/pallas_call | solution.py:262
  121.6 6.4 %ahead.1.before = f32[1280,768]{1,0:T(8,128)} custom-call(bf16[2048,512]{1,0:T(8,128)(2,1)} %get-tuple-element.38.gate_up, bf16[2048,256]{1,0:T(8,128)(2,1)} %get-tuple-element.39.down, bf16[640,640]{1,0:T(8,128)(2,1)S(1)} %bitcast.33, bf16[640,640]{1,0:T(8,128)(2,1)S(1)} %bitcast.28, bf16[640,640]{1,0:T(8,128)(2,1)S(1)} %collective-permute-done.refs_2_, ...), custom_call_target="tpu_custom_call" | custom-call | flops 2000000000 | bytes 12582912 | tf_op jit(solution)/shard_map/ahead/pallas_call | solution.py:289
  128.2 2.5 collective-permute-start.16
  130.7 1.2 collective-permute-done.14.refs_2_
  131.8 2.1 collective-permute-done.17.refs_5_
  133.9 3.4 %collective-permute-start.19 = (bf16[640,256]{1,0:T(8,128)(2,1)S(1)}, bf16[640,256]{1,0:T(8,128)(2,1)S(1)}, u32[]{:S(2)}, u32[]{:S(2)}) collective-permute-start(bf16[640,256]{1,0:T(8,128)(2,1)S(1)} %collective-permute-done.17.refs_5_), channel_id=1, source_target_pairs={{0,3},{1,0},{2,1},{3,2},{4,7},{5,4},{6,5},{7,6},{8,11},{9,8},{10,9... | collective-permute-start | bytes 983048 | tf_op jit(solution)/shard_map/ppermute | solution.py:601
  137.3 10.2 %expert.1 = (bf16[1280,256]{1,0:T(8,128)(2,1)}, bf16[1280,256]{1,0:T(8,128)(2,1)}, bf16[1280,256]{1,0:T(8,128)(2,1)}, bf16[4,1280,256]{2,1,0:T(8,128)(2,1)}) custom-call(bf16[1280,1792]{1,0:T(8,128)(2,1)} %bitcast.8.got_rows.got_cot, bf16[1280,1792]{1,0:T(8,128)(2,1)} %bitcast.8.got_rows.got_cot, bf16[640,640]{1,0:T(8,128)(2,1)} %collective-permute-done.4.far_top.refs_6_, ...), custom_call_target="tpu_custom_call" | custom-call | flops 5000000000 | bytes 16777216 | tf_op jit(solution)/shard_map/expert/pallas_call | solution.py:343
  147.9 8.9 %proj.1.kept_ref = bf16[2,4,16,64,256]{4,3,2,1,0:T(8,128)(2,1)} custom-call(s32[3]{0:T(128)S(1)} %pad_add_fusion.where_ref, bf16[1280,256]{1,0:T(8,128)(2,1)} %get-tuple-element.42.refs_8_.gate_cot, bf16[1280,256]{1,0:T(8,128)(2,1)} %get-tuple-element.43.refs_9_.up_cot, bf16[2048,256]{1,0:T(8,128)(2,1)} %bitcast.47, bf16[2048,256]{1,0:T(8,128)(2,1)} %bitcast.49, ...), custom_call_target="tpu_custom_call" | custom-call | flops 4000000000 | bytes 14680064 | tf_op jit(solution)/shard_map/proj/pallas_call | solution.py:472
  156.8 3.2 %slice_bitcast_fusion = bf16[4,16,64,256]{3,2,1,0:T(8,128)(2,1)} fusion(bf16[2,4,16,64,256]{4,3,2,1,0:T(8,128)(2,1)} %proj.1.kept_ref), kind=kLoop, calls=%fused_computation.1 | loop fusion | bytes 4194304 | tf_op jit(solution)/shard_map/squeeze | solution.py:688
  160.0 1.2 collective-permute-start.20
  161.2 9.5 %all-to-all-start.3 = ((bf16[128,40,256]{2,1,0:T(8,128)(2,1)}), bf16[128,40,256]{2,1,0:T(8,128)(2,1)S(1)}, u32[]{:S(2)}, u32[]{:S(2)}) async-start(bf16[128,40,256]{2,1,0:T(8,128)(2,1)} %bitcast.39), calls=%async_computation.3 | async-start | bytes 5242880 | tf_op jit(solution)/shard_map/all_to_all | solution.py:679
  170.7 3.7 %chipsum.1 = (bf16[16,64,256]{2,1,0:T(8,128)(2,1)}, bf16[8,64,256]{2,1,0:T(8,128)(2,1)}, bf16[8,64,256]{2,1,0:T(8,128)(2,1)}, bf16[8,64,256]{2,1,0:T(8,128)(2,1)...) custom-call(bf16[2,4,16,64,256]{4,3,2,1,0:T(8,128)(2,1)} %proj.1.kept_ref, ...), custom_call_target="tpu_custom_call" | custom-call | flops 10000000 | bytes 6291456 | tf_op jit(solution)/shard_map/chipsum/pallas_call | solution.py:498
  174.4 1.4 collective-permute-start.21
  175.8 1.3 collective-permute-start.23
  177.1 1.4 collective-permute-start.25
  178.6 28.5 %collective-permute-done.21 = bf16[8,64,256]{2,1,0:T(8,128)(2,1)S(1)} collective-permute-done((bf16[8,64,256]{2,1,0:T(8,128)(2,1)}, bf16[8,64,256]{2,1,0:T(8,128)(2,1)S(1)}, u32[]{:S(2)}, u32[]{:S(2)}) %collective-permute-start.21) | collective-permute-done | bytes 262176 | tf_op jit(solution)/shard_map/ppermute | solution.py:601
  207.1 1.0 add_convert_fusion.2
  208.2 1.7 add_convert_fusion.1
  209.9 2.7 %collective-permute-start.24 = (bf16[8,64,256]{2,1,0:T(8,128)(2,1)}, bf16[8,64,256]{2,1,0:T(8,128)(2,1)}, u32[]{:S(2)}, u32[]{:S(2)}) collective-permute-start(bf16[8,64,256]{2,1,0:T(8,128)(2,1)} %add_convert_fusion.1), channel_id=1, source_target_pairs={{0,3},{1,0},{2,1},{3,2},{4,7},{5,4},{6,5},{7,6},{8,11},{9,8},{10,9... | collective-permute-start | bytes 786440 | tf_op jit(solution)/shard_map/ppermute | solution.py:601
  212.6 1.5 fusion.4.base
  214.1 4.6 %scanned.1 = (bf16[512,256]{1,0:T(8,128)(2,1)}, f32[512,256]{1,0:T(8,128)}, f32[32,2,256]{2,1,0:T(2,128)}) custom-call(bf16[4,1280,256]{2,1,0:T(8,128)(2,1)S(1)} %bitcast.36, bf16[512,1280]{1,0:T(8,128)(2,1)} %get-tuple-element.55.sel, f32[512,256]{1,0:T(8,128)} %fusion.4.base, f32[512,256]{1,0:T(8,128)} %get-tuple-element.56.act, ...), custom_call_target="tpu_custom_call" | custom-call | flops 400000000 | bytes 8388608 | tf_op jit(solution)/shard_map/scanned/pallas_call | solution.py:554
  218.7 9.1 %all-to-all-start.4 = ((f32[32,2,256]{2,1,0:T(2,128)}), f32[32,2,256]{2,1,0:T(2,128)S(1)}, u32[]{:S(2)}, u32[]{:S(2)}) async-start(f32[32,2,256]{2,1,0:T(2,128)} %get-tuple-element.61), calls=%async_computation.4 | async-start | bytes 131072 | tf_op jit(solution)/shard_map/all_to_all | solution.py:707
  227.8 2.3 add_convert_fusion
  230.1 5.0 %all-to-all-done.4.pairs = f32[32,2,256]{2,1,0:T(2,128)S(1)} async-done(((f32[32,2,256]{2,1,0:T(2,128)}), f32[32,2,256]{2,1,0:T(2,128)S(1)}, u32[]{:S(2)}, u32[]{:S(2)}) %all-to-all-start.4) | async-done | bytes 65568 | tf_op jit(solution)/shard_map/all_to_all | solution.py:707
  235.1 3.6 %all-to-all-start.2 = ((bf16[16,64,256]{2,1,0:T(8,128)(2,1)}), bf16[16,64,256]{2,1,0:T(8,128)(2,1)S(1)}, u32[]{:S(2)}, u32[]{:S(2)}) async-start(bf16[16,64,256]{2,1,0:T(8,128)(2,1)} %add_convert_fusion), calls=%async_computation.2 | async-start | bytes 1048576 | tf_op jit(solution)/shard_map/all_to_all | solution.py:702
  238.7 6.8 %downgrads.1 = f32[1,256,2048]{2,1,0:T(8,128)} custom-call(s32[3]{0:T(128)S(1)} %pad_add_fusion.where_ref, bf16[1280,1792]{1,0:T(8,128)(2,1)} %bitcast.8.got_rows.got_cot, bf16[640,640]{1,0:T(8,128)(2,1)} %bitcast.34, bf16[640,640]{1,0:T(8,128)(2,1)} %bitcast.29, bf16[640,640]{1,0:T(8,128)(2,1)} %copy-done.2, ...), custom_call_target="tpu_custom_call" | custom-call | flops 1500000000 | bytes 11534336 | tf_op jit(solution)/shard_map/downgrads/pallas_call | solution.py:430
  245.5 8.1 %rowgrads.1 = (f32[1,2048,256]{2,1,0:T(8,128)}, f32[1,2048,256]{2,1,0:T(8,128)}) custom-call(s32[3]{0:T(128)S(1)} %pad_add_fusion.where_ref, bf16[1280,1792]{1,0:T(8,128)(2,1)} %bitcast.8.got_rows.got_cot, bf16[640,640]{1,0:T(8,128)(2,1)} %bitcast.35, bf16[640,640]{1,0:T(8,128)(2,1)} %bitcast.30, bf16[640,640]{1,0:T(8,128)(2,1)} %copy-done.2, ...), custom_call_target="tpu_custom_call" | custom-call | flops 3000000000 | bytes 11534336 | tf_op jit(solution)/shard_map/rowgrads/pallas_call | solution.py:409
  253.6 2.9 %final.1 = bf16[512,256]{1,0:T(8,128)(2,1)} custom-call(s32[3]{0:T(128)S(1)} %pad_add_fusion.where_ref, f32[32,2,256]{2,1,0:T(2,128)S(1)} %all-to-all-done.4.pairs, f32[512,256]{1,0:T(8,128)} %get-tuple-element.62.local, f32[512,256]{1,0:T(8,128)} %get-tuple-element.63.exp, f32[512,256]{1,0:T(8,128)} %get-tuple-element.64.ca, ...), custom_call_target="tpu_custom_call" | custom-call | flops 100000000 | bytes 4194304 | tf_op jit(solution)/shard_map/final/pallas_call | solution.py:589
  (80 shorter events, 5.5 us)
Async XLA Ops:
  5.4 9.8 %copy-start.23 = (s32[512,2]{0,1:T(2,128)S(1)}, s32[512,2]{0,1:T(2,128)}, u32[]{:S(2)}) copy-start(s32[512,2]{0,1:T(2,128)} %param.17) | copy-start | bytes 12292
  5.4 10.6 %copy-start.24 = (f32[2,512]{1,0:T(2,128)S(1)}, f32[2,512]{1,0:T(2,128)}, u32[]{:S(2)}) copy-start(f32[2,512]{1,0:T(2,128)} %param.27) | copy-start | bytes 12292
  5.4 11.5 %copy-start.25 = (f32[1024]{0:T(1024)S(1)}, f32[1024]{0:T(1024)}, u32[]{:S(2)}) copy-start(f32[1024]{0:T(1024)} %param.26) | copy-start | bytes 12292
  5.4 33.3 %all-to-all-start.1 = ((bf16[32,40,640]{2,1,0:T(8,128)(2,1)}), bf16[32,40,640]{2,1,0:T(8,128)(2,1)S(1)}, u32[]{:S(2)}, u32[]{:S(2)}) async-start(bf16[32,40,640]{2,1,0:T(8,128)(2,1)} %bitcast.37), calls=%async_computation.1 | async-start | bytes 3276800 | tf_op jit(solution)/shard_map/all_to_all | solution.py:641
  38.8 1.2 copy-start.18
  38.8 7.0 %copy-start.21 = (bf16[2048,256]{1,0:T(8,128)(2,1)S(1)}, bf16[2048,256]{1,0:T(8,128)(2,1)}, u32[]{:S(2)}) copy-start(bf16[2048,256]{1,0:T(8,128)(2,1)} %whole_own.1) | copy-start | bytes 3145732
  39.9 60.5 %all-to-all-start = ((bf16[32,40,1792]{2,1,0:T(8,128)(2,1)}), bf16[32,40,1792]{2,1,0:T(8,128)(2,1)}, u32[]{:S(2)}, u32[]{:S(2)}) async-start(bf16[32,40,1792]{2,1,0:T(8,128)(2,1)} %bitcast.38), calls=%async_computation | async-start | bytes 9175040 | tf_op jit(solution)/shard_map/all_to_all | solution.py:641
  45.8 48.6 %copy-start.16 = (bf16[512,2048]{1,0:T(8,128)(2,1)S(1)}, bf16[512,2048]{1,0:T(8,128)(2,1)}, u32[]{:S(2)}) copy-start(bf16[512,2048]{1,0:T(8,128)(2,1)} %refs_1_.3) | copy-start | bytes 6291460
  45.8 48.6 %copy-start.20 = (bf16[512,256]{1,0:T(8,128)(2,1)S(1)}, bf16[512,256]{1,0:T(8,128)(2,1)}, u32[]{:S(2)}) copy-start(bf16[512,256]{1,0:T(8,128)(2,1)} %get-tuple-element.37.refs_2_) | copy-start | bytes 786436
  45.8 14.5 %collective-permute-start.6 = (bf16[1024,256]{1,0:T(8,128)(2,1)S(1)}, bf16[1024,256]{1,0:T(8,128)(2,1)S(1)}, u32[]{:S(2)}, u32[]{:S(2)}) collective-permute-start(bf16[1024,256]{1,0:T(8,128)(2,1)S(1)} %constant_dynamic-slice_fusion), channel_id=1, source_target_pairs={{0,1},{1,2},{2,3},{3,0},{4,5},{5,6},{6,7},{7,4},{8,9},{9,10},{10,1... | collective-permute-start | bytes 1572872 | tf_op jit(solution)/shard_map/ppermute | solution.py:601
  47.1 13.3 %collective-permute-start.7 = (bf16[1024,256]{1,0:T(8,128)(2,1)S(1)}, bf16[1024,256]{1,0:T(8,128)(2,1)}, u32[]{:S(2)}, u32[]{:S(2)}) collective-permute-start(bf16[1024,256]{1,0:T(8,128)(2,1)S(1)} %constant_dynamic-slice_fusion), channel_id=1, source_target_pairs={{0,3},{1,0},{2,1},{3,2},{4,7},{5,4},{6,5},{7,6},{8,11},{9,8},{10,9... | collective-permute-start | bytes 1572872 | tf_op jit(solution)/shard_map/ppermute | solution.py:601
  50.1 71.5 %copy-start = (bf16[16,40,640]{2,1,0:T(8,128)(2,1)}, bf16[16,40,640]{2,1,0:T(8,128)(2,1)S(1)}, u32[]{:S(2)}) copy-start(bf16[16,40,640]{2,1,0:T(8,128)(2,1)S(1)} %get-tuple-element.70) | copy-start | bytes 2457604
  50.1 71.5 %copy-start.1 = (bf16[16,40,640]{2,1,0:T(8,128)(2,1)}, bf16[16,40,640]{2,1,0:T(8,128)(2,1)S(1)}, u32[]{:S(2)}) copy-start(bf16[16,40,640]{2,1,0:T(8,128)(2,1)S(1)} %get-tuple-element.71) | copy-start | bytes 2457604
  50.1 41.6 %collective-permute-start = (bf16[640,640]{1,0:T(8,128)(2,1)S(1)}, bf16[640,640]{1,0:T(8,128)(2,1)S(1)}, u32[]{:S(2)}, u32[]{:S(2)}) collective-permute-start(bf16[640,640]{1,0:T(8,128)(2,1)S(1)} %bitcast.31), channel_id=1, source_target_pairs={{0,1},{1,2},{2,3},{3,0},{4,5},{5,6},{6,7},{7,4},{8,9},{9,10},{10,1... | collective-permute-start | bytes 2457608 | tf_op jit(solution)/shard_map/ppermute | solution.py:601
  50.2 41.5 %collective-permute-start.3 = (bf16[640,640]{1,0:T(8,128)(2,1)S(1)}, bf16[640,640]{1,0:T(8,128)(2,1)S(1)}, u32[]{:S(2)}, u32[]{:S(2)}) collective-permute-start(bf16[640,640]{1,0:T(8,128)(2,1)S(1)} %bitcast.26), channel_id=1, source_target_pairs={{0,3},{1,0},{2,1},{3,2},{4,7},{5,4},{6,5},{7,6},{8,11},{9,8},{10,9... | collective-permute-start | bytes 2457608 | tf_op jit(solution)/shard_map/ppermute | solution.py:601
  60.3 23.2 %collective-permute-start.8 = (bf16[512,256]{1,0:T(8,128)(2,1)S(1)}, bf16[512,256]{1,0:T(8,128)(2,1)S(1)}, u32[]{:S(2)}, u32[]{:S(2)}) collective-permute-start(bf16[512,256]{1,0:T(8,128)(2,1)S(1)} %slice.38), channel_id=1, source_target_pairs={{0,1},{1,2},{2,3},{3,0},{4,5},{5,6},{6,7},{7,4},{8,9},{9,10},{10,1... | collective-permute-start | bytes 786440 | tf_op jit(solution)/shard_map/ppermute | solution.py:601
  61.3 24.0 %collective-permute-start.9 = (bf16[512,256]{1,0:T(8,128)(2,1)S(1)}, bf16[512,256]{1,0:T(8,128)(2,1)S(1)}, u32[]{:S(2)}, u32[]{:S(2)}) collective-permute-start(bf16[512,256]{1,0:T(8,128)(2,1)S(1)} %slice.39), channel_id=1, source_target_pairs={{0,3},{1,0},{2,1},{3,2},{4,7},{5,4},{6,5},{7,6},{8,11},{9,8},{10,9... | collective-permute-start | bytes 786440 | tf_op jit(solution)/shard_map/ppermute | solution.py:601
  64.1 24.2 %collective-permute-start.10 = (bf16[1024,256]{1,0:T(8,128)(2,1)S(1)}, bf16[1024,256]{1,0:T(8,128)(2,1)S(1)}, u32[]{:S(2)}, u32[]{:S(2)}) collective-permute-start(bf16[1024,256]{1,0:T(8,128)(2,1)S(1)} %collective-permute-done.6.refs_0_), channel_id=1, source_target_pairs={{0,4},{4,0},{1,5},{5,1},{2,6},{6,2},{3,7},{7,3},{8,12},{12,8},{9,1... | collective-permute-start | bytes 1572872 | tf_op jit(solution)/shard_map/ppermute | solution.py:618
  66.7 0.8 copy-start.4
  83.4 2.6 %collective-permute-start.12 = (bf16[512,256]{1,0:T(8,128)(2,1)S(1)}, bf16[512,256]{1,0:T(8,128)(2,1)S(1)}, u32[]{:S(2)}, u32[]{:S(2)}) collective-permute-start(bf16[512,256]{1,0:T(8,128)(2,1)S(1)} %collective-permute-done.8.refs_2_), channel_id=1, source_target_pairs={{0,4},{4,0},{1,5},{5,1},{2,6},{6,2},{3,7},{7,3},{8,12},{12,8},{9,1... | collective-permute-start | bytes 786440 | tf_op jit(solution)/shard_map/ppermute | solution.py:618
  84.6 0.7 copy-start.8
  85.3 1.9 collective-permute-start.13
  85.3 0.7 copy-start.10
  86.0 0.7 copy-start.12
  86.7 20.6 %collective-permute-start.1 = (bf16[640,640]{1,0:T(8,128)(2,1)S(1)}, bf16[640,640]{1,0:T(8,128)(2,1)}, u32[]{:S(2)}, u32[]{:S(2)}) collective-permute-start(bf16[640,640]{1,0:T(8,128)(2,1)S(1)} %bitcast.27), channel_id=1, source_target_pairs={{0,1},{1,2},{2,3},{3,0},{4,5},{5,6},{6,7},{7,4},{8,9},{9,10},{10,1... | collective-permute-start | bytes 2457608 | tf_op jit(solution)/shard_map/ppermute | solution.py:601
  87.2 0.7 copy-start.14
  87.9 13.7 %collective-permute-start.11 = (bf16[1024,256]{1,0:T(8,128)(2,1)}, bf16[1024,256]{1,0:T(8,128)(2,1)}, u32[]{:S(2)}, u32[]{:S(2)}) collective-permute-start(bf16[1024,256]{1,0:T(8,128)(2,1)} %collective-permute-done.7.refs_1_), channel_id=1, source_target_pairs={{0,4},{4,0},{1,5},{5,1},{2,6},{6,2},{3,7},{7,3},{8,12},{12,8},{9,1... | collective-permute-start | bytes 1572872 | tf_op jit(solution)/shard_map/ppermute | solution.py:618
  88.2 0.8 copy-start.6
  89.0 32.5 %collective-permute-start.2 = (bf16[640,640]{1,0:T(8,128)(2,1)S(1)}, bf16[640,640]{1,0:T(8,128)(2,1)}, u32[]{:S(2)}, u32[]{:S(2)}) collective-permute-start(bf16[640,640]{1,0:T(8,128)(2,1)S(1)} %bitcast.32), channel_id=1, source_target_pairs={{0,3},{1,0},{2,1},{3,2},{4,7},{5,4},{6,5},{7,6},{8,11},{9,8},{10,9... | collective-permute-start | bytes 2457608 | tf_op jit(solution)/shard_map/ppermute | solution.py:601
  91.7 29.9 %copy-start.2 = (bf16[640,640]{1,0:T(8,128)(2,1)}, bf16[640,640]{1,0:T(8,128)(2,1)S(1)}, u32[]{:S(2)}) copy-start(bf16[640,640]{1,0:T(8,128)(2,1)S(1)} %collective-permute-done.refs_2_) | copy-start | bytes 2457604
  91.7 36.5 %collective-permute-start.4 = (bf16[640,640]{1,0:T(8,128)(2,1)S(1)}, bf16[640,640]{1,0:T(8,128)(2,1)}, u32[]{:S(2)}, u32[]{:S(2)}) collective-permute-start(bf16[640,640]{1,0:T(8,128)(2,1)S(1)} %collective-permute-done.refs_2_), channel_id=1, source_target_pairs={{0,1},{1,2},{2,3},{3,0},{4,5},{5,6},{6,7},{7,4},{8,9},{9,10},{10,1... | collective-permute-start | bytes 2457608 | tf_op jit(solution)/shard_map/ppermute | solution.py:601
  91.7 29.9 %copy-start.3 = (bf16[640,640]{1,0:T(8,128)(2,1)}, bf16[640,640]{1,0:T(8,128)(2,1)S(1)}, u32[]{:S(2)}) copy-start(bf16[640,640]{1,0:T(8,128)(2,1)S(1)} %collective-permute-done.3.refs_5_) | copy-start | bytes 2457604
  91.7 45.6 %collective-permute-start.5 = (bf16[640,640]{1,0:T(8,128)(2,1)S(1)}, bf16[640,640]{1,0:T(8,128)(2,1)}, u32[]{:S(2)}, u32[]{:S(2)}) collective-permute-start(bf16[640,640]{1,0:T(8,128)(2,1)S(1)} %collective-permute-done.3.refs_5_), channel_id=1, source_target_pairs={{0,3},{1,0},{2,1},{3,2},{4,7},{5,4},{6,5},{7,6},{8,11},{9,8},{10,9... | collective-permute-start | bytes 2457608 | tf_op jit(solution)/shard_map/ppermute | solution.py:601
  101.6 30.2 %collective-permute-start.14 = (bf16[640,256]{1,0:T(8,128)(2,1)S(1)}, bf16[640,256]{1,0:T(8,128)(2,1)S(1)}, u32[]{:S(2)}, u32[]{:S(2)}) collective-permute-start(bf16[640,256]{1,0:T(8,128)(2,1)S(1)} %get-tuple-element.69.refs_0_), channel_id=1, source_target_pairs={{0,1},{1,2},{2,3},{3,0},{4,5},{5,6},{6,7},{7,4},{8,9},{9,10},{10,1... | collective-permute-start | bytes 983048 | tf_op jit(solution)/shard_map/ppermute | solution.py:601
  107.4 26.5 %collective-permute-start.17 = (bf16[640,256]{1,0:T(8,128)(2,1)S(1)}, bf16[640,256]{1,0:T(8,128)(2,1)S(1)}, u32[]{:S(2)}, u32[]{:S(2)}) collective-permute-start(bf16[640,256]{1,0:T(8,128)(2,1)S(1)} %get-tuple-element.68.refs_1_), channel_id=1, source_target_pairs={{0,3},{1,0},{2,1},{3,2},{4,7},{5,4},{6,5},{7,6},{8,11},{9,8},{10,9... | collective-permute-start | bytes 983048 | tf_op jit(solution)/shard_map/ppermute | solution.py:601
  108.6 1.0 copy-start.5
  109.7 1.0 copy-start.7
  110.7 0.9 copy-start.9
  111.6 0.9 copy-start.11
  112.6 0.9 copy-start.13
  113.5 0.9 copy-start.15
  128.0 19.5 %collective-permute-start.15 = (bf16[640,256]{1,0:T(8,128)(2,1)S(1)}, bf16[640,256]{1,0:T(8,128)(2,1)S(1)}, u32[]{:S(2)}, u32[]{:S(2)}) collective-permute-start(bf16[640,256]{1,0:T(8,128)(2,1)S(1)} %get-tuple-element.68.refs_1_), channel_id=1, source_target_pairs={{0,1},{1,2},{2,3},{3,0},{4,5},{5,6},{6,7},{7,4},{8,9},{9,10},{10,1... | collective-permute-start | bytes 983048 | tf_op jit(solution)/shard_map/ppermute | solution.py:601
  128.2 19.3 %collective-permute-start.16 = (bf16[640,256]{1,0:T(8,128)(2,1)S(1)}, bf16[640,256]{1,0:T(8,128)(2,1)S(1)}, u32[]{:S(2)}, u32[]{:S(2)}) collective-permute-start(bf16[640,256]{1,0:T(8,128)(2,1)S(1)} %get-tuple-element.69.refs_0_), channel_id=1, source_target_pairs={{0,3},{1,0},{2,1},{3,2},{4,7},{5,4},{6,5},{7,6},{8,11},{9,8},{10,9... | collective-permute-start | bytes 983048 | tf_op jit(solution)/shard_map/ppermute | solution.py:601
  131.8 15.7 %collective-permute-start.18 = (bf16[640,256]{1,0:T(8,128)(2,1)S(1)}, bf16[640,256]{1,0:T(8,128)(2,1)S(1)}, u32[]{:S(2)}, u32[]{:S(2)}) collective-permute-start(bf16[640,256]{1,0:T(8,128)(2,1)S(1)} %collective-permute-done.14.refs_2_), channel_id=1, source_target_pairs={{0,1},{1,2},{2,3},{3,0},{4,5},{5,6},{6,7},{7,4},{8,9},{9,10},{10,1... | collective-permute-start | bytes 983048 | tf_op jit(solution)/shard_map/ppermute | solution.py:601
  133.9 14.0 %collective-permute-start.19 = (bf16[640,256]{1,0:T(8,128)(2,1)S(1)}, bf16[640,256]{1,0:T(8,128)(2,1)S(1)}, u32[]{:S(2)}, u32[]{:S(2)}) collective-permute-start(bf16[640,256]{1,0:T(8,128)(2,1)S(1)} %collective-permute-done.17.refs_5_), channel_id=1, source_target_pairs={{0,3},{1,0},{2,1},{3,2},{4,7},{5,4},{6,5},{7,6},{8,11},{9,8},{10,9... | collective-permute-start | bytes 983048 | tf_op jit(solution)/shard_map/ppermute | solution.py:601
  160.0 10.7 %collective-permute-start.20 = (bf16[4,16,64,256]{3,2,1,0:T(8,128)(2,1)}, bf16[4,16,64,256]{3,2,1,0:T(8,128)(2,1)}, u32[]{:S(2)}, u32[]{:S(2)}) collective-permute-start(bf16[4,16,64,256]{3,2,1,0:T(8,128)(2,1)} %slice_bitcast_fusion), channel_id=1, source_target_pairs={{0,4},{4,0},{1,5},{5,1},{2,6},{6,2},{3,7},{7,3},{8,12},{12,8},{9,1... | collective-permute-start | bytes 6291464 | tf_op jit(solution)/shard_map/ppermute | solution.py:688
  161.2 52.9 %all-to-all-start.3 = ((bf16[128,40,256]{2,1,0:T(8,128)(2,1)}), bf16[128,40,256]{2,1,0:T(8,128)(2,1)S(1)}, u32[]{:S(2)}, u32[]{:S(2)}) async-start(bf16[128,40,256]{2,1,0:T(8,128)(2,1)} %bitcast.39), calls=%async_computation.3 | async-start | bytes 5242880 | tf_op jit(solution)/shard_map/all_to_all | solution.py:679
  170.7 41.9 %copy-start.17 = (bf16[512,2048]{1,0:T(8,128)(2,1)S(1)}, bf16[512,2048]{1,0:T(8,128)(2,1)}, u32[]{:S(2)}) copy-start(bf16[512,2048]{1,0:T(8,128)(2,1)} %refs_1_.3) | copy-start | bytes 6291460
  170.7 41.9 %copy-start.22 = (bf16[2048,256]{1,0:T(8,128)(2,1)S(1)}, bf16[2048,256]{1,0:T(8,128)(2,1)}, u32[]{:S(2)}) copy-start(bf16[2048,256]{1,0:T(8,128)(2,1)} %whole_own.1) | copy-start | bytes 3145732
  174.4 32.7 %collective-permute-start.21 = (bf16[8,64,256]{2,1,0:T(8,128)(2,1)}, bf16[8,64,256]{2,1,0:T(8,128)(2,1)S(1)}, u32[]{:S(2)}, u32[]{:S(2)}) collective-permute-start(bf16[8,64,256]{2,1,0:T(8,128)(2,1)} %get-tuple-element.48), channel_id=1, source_target_pairs={{0,1},{1,2},{2,3},{3,0},{4,5},{5,6},{6,7},{7,4},{8,9},{9,10},{10,1... | collective-permute-start | bytes 786440 | tf_op jit(solution)/shard_map/ppermute | solution.py:601
  175.8 32.4 %collective-permute-start.23 = (bf16[8,64,256]{2,1,0:T(8,128)(2,1)}, bf16[8,64,256]{2,1,0:T(8,128)(2,1)S(1)}, u32[]{:S(2)}, u32[]{:S(2)}) collective-permute-start(bf16[8,64,256]{2,1,0:T(8,128)(2,1)} %get-tuple-element.50), channel_id=1, source_target_pairs={{0,3},{1,0},{2,1},{3,2},{4,7},{5,4},{6,5},{7,6},{8,11},{9,8},{10,9... | collective-permute-start | bytes 786440 | tf_op jit(solution)/shard_map/ppermute | solution.py:601
  177.1 50.7 %collective-permute-start.25 = (bf16[8,64,256]{2,1,0:T(8,128)(2,1)}, bf16[8,64,256]{2,1,0:T(8,128)(2,1)}, u32[]{:S(2)}, u32[]{:S(2)}) collective-permute-start(bf16[8,64,256]{2,1,0:T(8,128)(2,1)} %get-tuple-element.51), channel_id=1, source_target_pairs={{0,3},{1,0},{2,1},{3,2},{4,7},{5,4},{6,5},{7,6},{8,11},{9,8},{10,9... | collective-permute-start | bytes 786440 | tf_op jit(solution)/shard_map/ppermute | solution.py:601
  178.5 49.3 %collective-permute-start.26 = (bf16[8,64,256]{2,1,0:T(8,128)(2,1)}, bf16[8,64,256]{2,1,0:T(8,128)(2,1)}, u32[]{:S(2)}, u32[]{:S(2)}) collective-permute-start(bf16[8,64,256]{2,1,0:T(8,128)(2,1)} %get-tuple-element.52), channel_id=1, source_target_pairs={{0,1},{1,2},{2,3},{3,0},{4,5},{5,6},{6,7},{7,4},{8,9},{9,10},{10,1... | collective-permute-start | bytes 786440 | tf_op jit(solution)/shard_map/ppermute | solution.py:601
  208.1 19.7 %collective-permute-start.22 = (bf16[8,64,256]{2,1,0:T(8,128)(2,1)S(1)}, bf16[8,64,256]{2,1,0:T(8,128)(2,1)}, u32[]{:S(2)}, u32[]{:S(2)}) collective-permute-start(bf16[8,64,256]{2,1,0:T(8,128)(2,1)S(1)} %add_convert_fusion.2), channel_id=1, source_target_pairs={{0,1},{1,2},{2,3},{3,0},{4,5},{5,6},{6,7},{7,4},{8,9},{9,10},{10,1... | collective-permute-start | bytes 786440 | tf_op jit(solution)/shard_map/ppermute | solution.py:601
  209.9 17.9 %collective-permute-start.24 = (bf16[8,64,256]{2,1,0:T(8,128)(2,1)}, bf16[8,64,256]{2,1,0:T(8,128)(2,1)}, u32[]{:S(2)}, u32[]{:S(2)}) collective-permute-start(bf16[8,64,256]{2,1,0:T(8,128)(2,1)} %add_convert_fusion.1), channel_id=1, source_target_pairs={{0,3},{1,0},{2,1},{3,2},{4,7},{5,4},{6,5},{7,6},{8,11},{9,8},{10,9... | collective-permute-start | bytes 786440 | tf_op jit(solution)/shard_map/ppermute | solution.py:601
  214.1 13.7 %copy-start.19 = (bf16[16,64,256]{2,1,0:T(8,128)(2,1)S(1)}, bf16[16,64,256]{2,1,0:T(8,128)(2,1)}, u32[]{:S(2)}) copy-start(bf16[16,64,256]{2,1,0:T(8,128)(2,1)} %get-tuple-element.53) | copy-start | bytes 1572868
  218.7 16.4 %all-to-all-start.4 = ((f32[32,2,256]{2,1,0:T(2,128)}), f32[32,2,256]{2,1,0:T(2,128)S(1)}, u32[]{:S(2)}, u32[]{:S(2)}) async-start(f32[32,2,256]{2,1,0:T(2,128)} %get-tuple-element.61), calls=%async_computation.4 | async-start | bytes 131072 | tf_op jit(solution)/shard_map/all_to_all | solution.py:707
  235.1 21.4 %all-to-all-start.2 = ((bf16[16,64,256]{2,1,0:T(8,128)(2,1)}), bf16[16,64,256]{2,1,0:T(8,128)(2,1)S(1)}, u32[]{:S(2)}, u32[]{:S(2)}) async-start(bf16[16,64,256]{2,1,0:T(8,128)(2,1)} %add_convert_fusion), calls=%async_computation.2 | async-start | bytes 1048576 | tf_op jit(solution)/shard_map/all_to_all | solution.py:702
where the time goes:
time: 258 us; the launch traced here: 257 us
  Pallas kernels  78.5 us (30%)
  waiting for transfers between devices  74.9 us (29%)
  starting transfers between devices  72.5 us (28%)
  local copies, waits for them, and re-layouts  20.1 us (8%)
  other arithmetic  6.37 us (2%)
  matrix products  3.76 us (1%)
    ppermute x22, waiting for transfers between devices, shifted(): return lax.ppermute(piece, 'tp', [(i, (i + by) % 4) for i in range(4)])  60 us
    ppermute x22, starting transfers between devices, shifted(): return lax.ppermute(piece, 'tp', [(i, (i + by) % 4) for i in range(4)])  29.6 us
    all_to_all x2, starting transfers between devices, exchanged(): lax.all_to_all(rows.reshape(sources, capacity, -1), sp_axes, 0, 0, tiled=...  15.5 us
    unnamed x54, local copies, waits for them, and re-layouts  13.2 us
    pallas_call x2, Pallas kernels, build(): pl.pallas_call(functools.partial(build_kernel, capacity=capacity, group=g...  11.5 us
    pallas_call x1, Pallas kernels, expert(): pl.pallas_call(functools.partial(expert_kernel, row_part=row_part), out_s...  10.2 us
    all_to_all x2, waiting for transfers between devices, exchanged(): lax.all_to_all(rows.reshape(sources, capacity, -1), sp_axes, 0, 0, tiled=...  9.86 us
    all_to_all x1, starting transfers between devices, per_device(): lax.all_to_all(mix.reshape(4 * sources, capacity, -1), ('tp', *sp_axes),...  9.46 us
  transfers between devices with their start and end apart: 32, of which 10 were waited for; matrix products, arithmetic and copies ran while one was open for 6% of the time, Pallas kernels for 25%

commit v1 on v0

--- a/solution.py
+++ b/solution.py
@@ -449,11 +449,8 @@
     core = where_ref[1]
     first = ((0,), (0,))
     for n, step in enumerate(ring_steps):
-        top, bottom = pieces[2 * n], pieces[2 * n + 1]
-        half = top.shape[0]
         push_gate, push_up = (
-            (dot(cot[:half, :], top[...], first) + dot(cot[half:, :], bottom[...], first)).astype(BF16)
-            for cot in (gate_cot, up_cot)
+            dot(cot[...], pieces[n][...], first).astype(BF16) for cot in (gate_cot, up_cot)
         )
         term = dot(w_gate[...], push_gate) + dot(w_up[...], push_up)
         if step == 0:
@@ -480,24 +477,16 @@
     )(position, *kept(args[1:6]), *pieces)
 
 
-def chip_kernel(kept_ref, other, out_own, *outs):
-    half = out_own.shape[0] // 2
-    out_own[...] = (kept_ref[0, 0].astype(F32) + other[0].astype(F32)).astype(BF16)
-    for n in range(6):
-        lines = slice((n % 2) * half, (n % 2 + 1) * half)
-        at = 1 + n // 2
-        outs[n][...] = (
-            kept_ref[0, at, lines].astype(F32) + other[at, lines].astype(F32)
-        ).astype(BF16)
+def chip_kernel(kept_ref, other, *outs):
+    for n, out in enumerate(outs):
+        out[...] = (kept_ref[0, n].astype(F32) + other[n].astype(F32)).astype(BF16)
 
 
 def chip_sum(parts, other):
-    groups, lines, width = other.shape[1:]
-    half = made((groups // 2, lines, width), BF16)
-    outs = (made((groups, lines, width), BF16),) + (half,) * 6
+    out = made(other.shape[1:], BF16)
     return pl.pallas_call(
         chip_kernel,
-        out_shape=outs,
+        out_shape=(out,) * other.shape[0],
         grid=(1,),
         in_specs=[
             pl.BlockSpec(
@@ -505,7 +494,7 @@
             ),
             whole(other.shape),
         ],
-        out_specs=[whole(o.shape) for o in outs],
+        out_specs=[whole(out.shape)] * other.shape[0],
         compiler_params=params(16),
         cost_estimate=cost(10**7, 6 * 2**20),
         name="chipsum",
@@ -608,6 +597,10 @@
     return top, bottom, left_top, left_bottom, right_top, right_bottom, far_top, far_bottom
 
 
+def across(own):
+    return own, shifted(own, 1), shifted(own, -1), shifted(own, 2)
+
+
 def shared_ring_gather(own, core):
     half = own.shape[0] // 2
     mine = lax.dynamic_slice_in_dim(own, core * half, half, 0)
@@ -682,23 +675,13 @@
     grad_gate, grad_up = row_grads(position, got, pieces, gate_cot, up_cot, width, row_part)
     grad_down = down_grads(position, got, pieces, hidden, width, row_part, cot_part)
     start = row_rest + cot_rest
-    recs = ring_gather(got[: slots // 2, start:], got[slots // 2 :, start:])
+    recs = across(got[:, start:])
     lines = width // sources
     parts = proj(position, gate_cot, up_cot, w_gate, w_up, local_proj, recs, lines)
     other = lax.ppermute(parts[1], "core", [(0, 1), (1, 0)])
-    own, left_top, left_bottom, right_top, right_bottom, far_top, far_bottom = chip_sum(
-        parts, other
-    )
-    through_top, through_bottom = shifted(far_top, 1), shifted(far_bottom, -1)
-    from_left, from_right = shifted(right_bottom, 1), shifted(left_top, -1)
-    both_top = (right_top.astype(F32) + through_top.astype(F32)).astype(BF16)
-    both_bottom = (left_bottom.astype(F32) + through_bottom.astype(F32)).astype(BF16)
-    last_top, last_bottom = shifted(both_top, 1), shifted(both_bottom, -1)
-    arriving = (
-        jnp.concatenate([last_top, last_bottom], axis=0).astype(F32)
-        + jnp.concatenate([from_right, from_left], axis=0).astype(F32)
-        + own.astype(F32)
-    ).astype(BF16)
+    own, left, right, far = chip_sum(parts, other)
+    terms = (shifted(right, 1), shifted(left, -1), shifted(far, 2))
+    arriving = (sum(t.astype(F32) for t in terms) + own.astype(F32)).astype(BF16)
     arrived = lax.all_to_all(arriving, "sq", 0, 0, tiled=True)
     grad_out_proj = arrived.astype(F32).sum(axis=0)
     gate_input_grad, local, pair = scanned(

time: 258 us -> 232 us (0.90)
  local copies, waits for them, and re-layouts: 20.1 us -> 5.68 us
  starting transfers between devices: 72.5 us -> 66.2 us
  waiting for transfers between devices: 74.9 us -> 72.3 us
    unnamed x54 -> x28, local copies, waits for them, and re-layouts: 13.2 us -> 1.78 us
    ppermute x22 -> x16, starting transfers between devices: 29.6 us -> 21 us  [shifted(): return lax.ppermute(piece, 'tp', [(i, (i + by) % 4) for i in range(4)])]
    all_to_all x1, waiting for transfers between devices: 0.01 us -> 7.28 us  [per_device(): lax.all_to_all(mix.reshape(4 * sources, capacity, -1), ('tp', *sp_axes),...]
    ppermute x22 -> x16, waiting for transfers between devices: 60 us -> 54.1 us  [shifted(): return lax.ppermute(piece, 'tp', [(i, (i + by) % 4) for i in range(4)])]
    all_to_all x1, waiting for transfers between devices: 5.02 us -> 0.01 us  [per_device(): pairs = lax.all_to_all(pair, sp_axes, 0, 0, tiled=True)]
    all_to_all x1, starting transfers between devices: 9.11 us -> 5.01 us  [per_device(): pairs = lax.all_to_all(pair, sp_axes, 0, 0, tiled=True)]
    all_to_all x2, waiting for transfers between devices: 9.86 us -> 6.04 us  [exchanged(): lax.all_to_all(rows.reshape(sources, capacity, -1), sp_axes, 0, 0, tiled=...]
    ppermute x1, waiting for transfers between devices: 0.01 us -> 3.79 us  [per_device(): other = lax.ppermute(parts[1], 'core', [(0, 1), (1, 0)])]
  transfers between devices with their start and end apart: 32 -> 26, of which waited for: 10 -> 10; matrix products, arithmetic and copies ran while one was open for 6% -> 5% of each run, Pallas kernels for 25% -> 32%
where the time goes in v1:
time: 232 us; the launch traced here: 231 us
  Pallas kernels  77.9 us (34%)
  waiting for transfers between devices  72.3 us (31%)
  starting transfers between devices  66.2 us (29%)
  local copies, waits for them, and re-layouts  5.68 us (2%)
  other arithmetic  3.9 us (2%)
  matrix products  3.76 us (2%)
    ppermute x16, waiting for transfers between devices, shifted(): return lax.ppermute(piece, 'tp', [(i, (i + by) % 4) for i in range(4)])  54.1 us
    ppermute x16, starting transfers between devices, shifted(): return lax.ppermute(piece, 'tp', [(i, (i + by) % 4) for i in range(4)])  21 us
    all_to_all x2, starting transfers between devices, exchanged(): lax.all_to_all(rows.reshape(sources, capacity, -1), sp_axes, 0, 0, tiled=...  15.7 us
    pallas_call x2, Pallas kernels, build(): pl.pallas_call(functools.partial(build_kernel, capacity=capacity, group=g...  11.5 us
    all_to_all x1, starting transfers between devices, per_device(): lax.all_to_all(mix.reshape(4 * sources, capacity, -1), ('tp', *sp_axes),...  11.3 us
    pallas_call x1, Pallas kernels, expert(): pl.pallas_call(functools.partial(expert_kernel, row_part=row_part), out_s...  10.2 us
    pallas_call x1, Pallas kernels, proj(): pl.pallas_call(proj_kernel, out_shape=out, in_specs=[SMEM] + [whole(a.sha...  9.31 us
    pallas_call x1, Pallas kernels, early(): pl.pallas_call(functools.partial(early_kernel, capacity=capacity, experts...  8.37 us
  transfers between devices with their start and end apart: 26, of which 10 were waited for; matrix products, arithmetic and copies ran while one was open for 5% of the time, Pallas kernels for 32%

profile of v1, /device:TPU:1, one launch (start us, length us, event | category | flops | bytes accessed | tf_op | source)
XLA Modules:
  0.0 230.7 jit_solution(13100374898883433605)
XLA Ops:
  0.6 0.1 pad_add_fusion.where_ref
  0.7 4.7 %shard_map.191 = bf16[1280,640]{1,0:T(8,128)(2,1)} custom-call(s32[3]{0:T(128)S(1)} %pad_add_fusion.where_ref, s32[2,512]{1,0:T(2,128)} %bitcast.41, f32[2,512]{1,0:T(2,128)} %bitcast.43, bf16[512,2048]{1,0:T(8,128)(2,1)} %refs_0_.3, bf16[512,2048]{1,0:T(8,128)(2,1)} %refs_1_.3), custom_call_target="tpu_custom_call" | custom-call | flops 896000000 | bytes 3200000 | tf_op jit(solution)/shard_map/pallas_call | solution.py:196
  5.4 9.7 %all-to-all-start.1 = ((bf16[32,40,640]{2,1,0:T(8,128)(2,1)}), bf16[32,40,640]{2,1,0:T(8,128)(2,1)S(1)}, u32[]{:S(2)}, u32[]{:S(2)}) async-start(bf16[32,40,640]{2,1,0:T(8,128)(2,1)} %bitcast.37), calls=%async_computation.1 | async-start | bytes 3276800 | tf_op jit(solution)/shard_map/all_to_all | solution.py:634
  15.2 0.9 copy.22.ids
  16.0 0.9 copy.21
  16.9 0.6 fusion.1.rates
  17.5 8.4 %early.1 = (bf16[512,256]{1,0:T(8,128)(2,1)}, f32[512,256]{1,0:T(8,128)}, f32[512,256]{1,0:T(8,128)}, f32[512,256]{1,0:T(8,128)}, f32[512,256]{1,0:T(8,128)}, /*...) custom-call(s32[3]{0:T(128)S(1)} %pad_add_fusion.where_ref, ...), custom_call_target="tpu_custom_call" | custom-call | flops 3000000000 | bytes 8388608 | tf_op jit(solution)/shard_map/early/pallas_call | solution.py:142
  25.9 6.8 %shard_map.190 = bf16[1280,1792]{1,0:T(8,128)(2,1)} custom-call(s32[3]{0:T(128)S(1)} %pad_add_fusion.where_ref, s32[2,512]{1,0:T(2,128)} %bitcast.42, f32[2,512]{1,0:T(2,128)} %bitcast.44, bf16[512,2048]{1,0:T(8,128)(2,1)} %refs_0_.3, bf16[512,2048]{1,0:T(8,128)(2,1)} %refs_1_.3, bf16[512,256]{1,0:T(8,128)(2,1)} %get-tuple-element.34.refs_2_), custom_call_target="tpu_custom_call" | custom-call | flops 2508800000 | bytes 8960000 | tf_op jit(solution)/shard_map/pallas_call | solution.py:196
  32.7 6.0 %all-to-all-done.1 = bf16[32,40,640]{2,1,0:T(8,128)(2,1)S(1)} async-done(((bf16[32,40,640]{2,1,0:T(8,128)(2,1)}), bf16[32,40,640]{2,1,0:T(8,128)(2,1)S(1)}, u32[]{:S(2)}, u32[]{:S(2)}) %all-to-all-start.1) | async-done | bytes 1638432 | tf_op jit(solution)/shard_map/all_to_all | solution.py:634
  38.8 5.9 %all-to-all-start = ((bf16[32,40,1792]{2,1,0:T(8,128)(2,1)}), bf16[32,40,1792]{2,1,0:T(8,128)(2,1)}, u32[]{:S(2)}, u32[]{:S(2)}) async-start(bf16[32,40,1792]{2,1,0:T(8,128)(2,1)} %bitcast.38), calls=%async_computation | async-start | bytes 9175040 | tf_op jit(solution)/shard_map/all_to_all | solution.py:634
  44.8 0.0 copy-start.4
  44.8 0.0 copy-start.7
  44.8 1.3 collective-permute-start.6
  46.1 1.5 collective-permute-start.7
  47.5 0.1 fusion.2
  47.7 0.1 collective-permute-start
  47.8 2.7 %collective-permute-start.3 = (bf16[640,640]{1,0:T(8,128)(2,1)S(1)}, bf16[640,640]{1,0:T(8,128)(2,1)S(1)}, u32[]{:S(2)}, u32[]{:S(2)}) collective-permute-start(bf16[640,640]{1,0:T(8,128)(2,1)S(1)} %bitcast.26), channel_id=1, source_target_pairs={{0,3},{1,0},{2,1},{3,2},{4,7},{5,4},{6,5},{7,6},{8,11},{9,8},{10,9... | collective-permute-start | bytes 2457608 | tf_op jit(solution)/shard_map/ppermute | solution.py:590
  50.4 8.8 %collective-permute-done.6.refs_0_ = bf16[1024,256]{1,0:T(8,128)(2,1)S(1)} collective-permute-done((bf16[1024,256]{1,0:T(8,128)(2,1)S(1)}, bf16[1024,256]{1,0:T(8,128)(2,1)S(1)}, u32[]{:S(2)}, u32[]{:S(2)}) %collective-permute-start.6) | collective-permute-done | bytes 524320 | tf_op jit(solution)/shard_map/ppermute | solution.py:590
  59.3 0.1 collective-permute-start.8
  59.3 0.0 collective-permute-done.7.refs_1_
  59.4 2.7 %collective-permute-start.9 = (bf16[512,256]{1,0:T(8,128)(2,1)S(1)}, bf16[512,256]{1,0:T(8,128)(2,1)S(1)}, u32[]{:S(2)}, u32[]{:S(2)}) collective-permute-start(bf16[512,256]{1,0:T(8,128)(2,1)S(1)} %slice.35), channel_id=1, source_target_pairs={{0,3},{1,0},{2,1},{3,2},{4,7},{5,4},{6,5},{7,6},{8,11},{9,8},{10,9... | collective-permute-start | bytes 786440 | tf_op jit(solution)/shard_map/ppermute | solution.py:590
  62.1 2.6 %collective-permute-start.10 = (bf16[1024,256]{1,0:T(8,128)(2,1)S(1)}, bf16[1024,256]{1,0:T(8,128)(2,1)S(1)}, u32[]{:S(2)}, u32[]{:S(2)}) collective-permute-start(bf16[1024,256]{1,0:T(8,128)(2,1)S(1)} %collective-permute-done.6.refs_0_), channel_id=1, source_target_pairs={{0,4},{4,0},{1,5},{5,1},{2,6},{6,2},{3,7},{7,3},{8,12},{12,8},{9,1... | collective-permute-start | bytes 1572872 | tf_op jit(solution)/shard_map/ppermute | solution.py:611
  64.7 17.7 %collective-permute-done.8.refs_2_ = bf16[512,256]{1,0:T(8,128)(2,1)S(1)} collective-permute-done((bf16[512,256]{1,0:T(8,128)(2,1)S(1)}, bf16[512,256]{1,0:T(8,128)(2,1)S(1)}, u32[]{:S(2)}, u32[]{:S(2)}) %collective-permute-start.8) | collective-permute-done | bytes 262176 | tf_op jit(solution)/shard_map/ppermute | solution.py:590
  82.4 1.2 collective-permute-start.12
  83.6 0.0 collective-permute-start.13
  83.6 1.2 collective-permute-done.12.refs_6_
  84.7 0.4 collective-permute-start.11
  85.1 0.0 collective-permute-done.13.refs_7_
  85.1 0.8 collective-permute-start.1
  86.0 1.8 collective-permute-start.2
  87.8 2.7 %collective-permute-start.5 = (bf16[640,640]{1,0:T(8,128)(2,1)S(1)}, bf16[640,640]{1,0:T(8,128)(2,1)}, u32[]{:S(2)}, u32[]{:S(2)}) collective-permute-start(bf16[640,640]{1,0:T(8,128)(2,1)S(1)} %collective-permute-done.3.refs_5_), channel_id=1, source_target_pairs={{0,3},{1,0},{2,1},{3,2},{4,7},{5,4},{6,5},{7,6},{8,11},{9,8},{10,9... | collective-permute-start | bytes 2457608 | tf_op jit(solution)/shard_map/ppermute | solution.py:590
  90.5 2.2 convolution_bitcast_fusion.local
  92.7 6.8 %folded.1 = (bf16[2048,512]{1,0:T(8,128)(2,1)}, bf16[2048,256]{1,0:T(8,128)(2,1)}, bf16[4,256,256]{2,1,0:T(8,128)(2,1)}, bf16[4,256,256]{2,1,0:T(8,128)(2,1)}) custom-call(s32[3]{0:T(128)S(1)} %pad_add_fusion.where_ref, bf16[2048,256]{1,0:T(8,128)(2,1)} %bitcast.46, bf16[2048,256]{1,0:T(8,128)(2,1)} %bitcast.48, bf16[256,2048]{1,0:T(8,128)(2,1)} %bitcast.45, ...), custom_call_target="tpu_custom_call" | custom-call | flops 4000000000 | bytes 7340032 | tf_op jit(solution)/shard_map/folded/pallas_call | solution.py:262
  99.5 2.0 slice.36.refs_0_
  101.5 1.1 collective-permute-start.14
  102.6 3.2 %collective-permute-done.1.refs_3_ = bf16[640,640]{1,0:T(8,128)(2,1)} collective-permute-done((bf16[640,640]{1,0:T(8,128)(2,1)S(1)}, bf16[640,640]{1,0:T(8,128)(2,1)}, u32[]{:S(2)}, u32[]{:S(2)}) %collective-permute-start.1) | collective-permute-done | bytes 819232 | tf_op jit(solution)/shard_map/ppermute | solution.py:590
  105.9 1.1 collective-permute-start.15
  107.0 0.9 collective-permute-start.16
  107.9 6.3 %ahead.1.before = f32[1280,768]{1,0:T(8,128)} custom-call(bf16[2048,512]{1,0:T(8,128)(2,1)} %get-tuple-element.35.gate_up, bf16[2048,256]{1,0:T(8,128)(2,1)} %get-tuple-element.36.down, bf16[640,640]{1,0:T(8,128)(2,1)S(1)} %bitcast.33, bf16[640,640]{1,0:T(8,128)(2,1)S(1)} %bitcast.28, bf16[640,640]{1,0:T(8,128)(2,1)S(1)} %collective-permute-done.refs_2_, ...), custom_call_target="tpu_custom_call" | custom-call | flops 2000000000 | bytes 12582912 | tf_op jit(solution)/shard_map/ahead/pallas_call | solution.py:289
  114.2 9.3 %collective-permute-done.4.far_top.refs_6_ = bf16[640,640]{1,0:T(8,128)(2,1)} collective-permute-done((bf16[640,640]{1,0:T(8,128)(2,1)S(1)}, bf16[640,640]{1,0:T(8,128)(2,1)}, u32[]{:S(2)}, u32[]{:S(2)}) %collective-permute-start.4) | collective-permute-done | bytes 819232 | tf_op jit(solution)/shard_map/ppermute | solution.py:590
  123.4 10.2 %expert.1 = (bf16[1280,256]{1,0:T(8,128)(2,1)}, bf16[1280,256]{1,0:T(8,128)(2,1)}, bf16[1280,256]{1,0:T(8,128)(2,1)}, bf16[4,1280,256]{2,1,0:T(8,128)(2,1)}) custom-call(bf16[1280,1792]{1,0:T(8,128)(2,1)} %bitcast.8.got_rows.got_cot, bf16[1280,1792]{1,0:T(8,128)(2,1)} %bitcast.8.got_rows.got_cot, bf16[640,640]{1,0:T(8,128)(2,1)} %collective-permute-done.4.far_top.refs_6_, ...), custom_call_target="tpu_custom_call" | custom-call | flops 5000000000 | bytes 16777216 | tf_op jit(solution)/shard_map/expert/pallas_call | solution.py:343
  133.6 11.3 %all-to-all-start.3 = ((bf16[128,40,256]{2,1,0:T(8,128)(2,1)}), bf16[128,40,256]{2,1,0:T(8,128)(2,1)S(1)}, u32[]{:S(2)}, u32[]{:S(2)}) async-start(bf16[128,40,256]{2,1,0:T(8,128)(2,1)} %bitcast.39), calls=%async_computation.3 | async-start | bytes 5242880 | tf_op jit(solution)/shard_map/all_to_all | solution.py:672
  144.9 7.4 %collective-permute-done.16.refs_3_ = bf16[1280,256]{1,0:T(8,128)(2,1)} collective-permute-done((bf16[1280,256]{1,0:T(8,128)(2,1)}, bf16[1280,256]{1,0:T(8,128)(2,1)}, u32[]{:S(2)}, u32[]{:S(2)}) %collective-permute-start.16) | collective-permute-done | bytes 655392 | tf_op jit(solution)/shard_map/ppermute | solution.py:590
  152.4 9.3 %proj.1.kept_ref = bf16[2,4,16,64,256]{4,3,2,1,0:T(8,128)(2,1)} custom-call(s32[3]{0:T(128)S(1)} %pad_add_fusion.where_ref, bf16[1280,256]{1,0:T(8,128)(2,1)} %get-tuple-element.39.refs_8_.gate_cot, bf16[1280,256]{1,0:T(8,128)(2,1)} %get-tuple-element.40.refs_9_.up_cot, bf16[2048,256]{1,0:T(8,128)(2,1)} %bitcast.47, bf16[2048,256]{1,0:T(8,128)(2,1)} %bitcast.49, ...), custom_call_target="tpu_custom_call" | custom-call | flops 4000000000 | bytes 14680064 | tf_op jit(solution)/shard_map/proj/pallas_call | solution.py:469
  161.7 1.7 slice_bitcast_fusion
  163.4 0.0 copy-start.5
  163.4 0.0 copy-start.9
  163.4 2.4 %collective-permute-start.17 = (bf16[4,16,64,256]{3,2,1,0:T(8,128)(2,1)S(1)}, bf16[4,16,64,256]{3,2,1,0:T(8,128)(2,1)S(1)}, u32[]{:S(2)}, u32[]{:S(2)}) collective-permute-start(bf16[4,16,64,256]{3,2,1,0:T(8,128)(2,1)S(1)} %slice_bitcast_fusion), channel_id=1, source_target_pairs={{0,4},{4,0},{1,5},{5,1},{2,6},{6,2},{3,7},{7,3},{8,12},{12,8},{9,1... | collective-permute-start | bytes 6291464 | tf_op jit(solution)/shard_map/ppermute | solution.py:681
  165.8 3.8 %collective-permute-done.17.other = bf16[4,16,64,256]{3,2,1,0:T(8,128)(2,1)S(1)} collective-permute-done((bf16[4,16,64,256]{3,2,1,0:T(8,128)(2,1)S(1)}, bf16[4,16,64,256]{3,2,1,0:T(8,128)(2,1)S(1)}, u32[]{:S(2)}, u32[]{:S(2)}) %collective-permute-start.17) | collective-permute-done | bytes 2097184 | tf_op jit(solution)/shard_map/ppermute | solution.py:681
  169.6 3.1 %chipsum.1 = (bf16[16,64,256]{2,1,0:T(8,128)(2,1)}, bf16[16,64,256]{2,1,0:T(8,128)(2,1)}, bf16[16,64,256]{2,1,0:T(8,128)(2,1)}, bf16[16,64,256]{2,1,0:T(8,128)(2,1)}) custom-call(bf16[2,4,16,64,256]{4,3,2,1,0:T(8,128)(2,1)} %proj.1.kept_ref, bf16[4,16,64,256]{3,2,1,0:T(8,128)(2,1)S(1)} %collective-permute-done.17.other), custom_call_target="tpu_custom_call" | custom-call | flops 10000000 | bytes 6291456 | tf_op jit(solution)/shard_map/chipsum/pallas_call | solution.py:487
  172.6 1.1 collective-permute-start.18
  173.8 2.0 collective-permute-start.19
  175.7 1.2 collective-permute-start.20
  176.9 1.5 fusion.3.base
  178.4 7.3 %all-to-all-done.3 = bf16[128,40,256]{2,1,0:T(8,128)(2,1)S(1)} async-done(((bf16[128,40,256]{2,1,0:T(8,128)(2,1)}), bf16[128,40,256]{2,1,0:T(8,128)(2,1)S(1)}, u32[]{:S(2)}, u32[]{:S(2)}) %all-to-all-start.3) | async-done | bytes 2621472 | tf_op jit(solution)/shard_map/all_to_all | solution.py:672
  185.7 4.6 %scanned.1 = (bf16[512,256]{1,0:T(8,128)(2,1)}, f32[512,256]{1,0:T(8,128)}, f32[32,2,256]{2,1,0:T(2,128)}) custom-call(bf16[4,1280,256]{2,1,0:T(8,128)(2,1)S(1)} %bitcast.36, bf16[512,1280]{1,0:T(8,128)(2,1)} %get-tuple-element.49.sel, f32[512,256]{1,0:T(8,128)} %fusion.3.base, f32[512,256]{1,0:T(8,128)} %get-tuple-element.50.act, ...), custom_call_target="tpu_custom_call" | custom-call | flops 400000000 | bytes 8388608 | tf_op jit(solution)/shard_map/scanned/pallas_call | solution.py:543
  190.3 5.0 %all-to-all-start.4 = ((f32[32,2,256]{2,1,0:T(2,128)}), f32[32,2,256]{2,1,0:T(2,128)S(1)}, u32[]{:S(2)}, u32[]{:S(2)}) async-start(f32[32,2,256]{2,1,0:T(2,128)} %get-tuple-element.55), calls=%async_computation.4 | async-start | bytes 131072 | tf_op jit(solution)/shard_map/all_to_all | solution.py:690
  195.3 7.6 %collective-permute-done.20 = bf16[16,64,256]{2,1,0:T(8,128)(2,1)} collective-permute-done((bf16[16,64,256]{2,1,0:T(8,128)(2,1)}, bf16[16,64,256]{2,1,0:T(8,128)(2,1)}, u32[]{:S(2)}, u32[]{:S(2)}) %collective-permute-start.20) | collective-permute-done | bytes 524320 | tf_op jit(solution)/shard_map/ppermute | solution.py:590
  202.9 2.5 %add_convert_fusion = bf16[16,64,256]{2,1,0:T(8,128)(2,1)} fusion(bf16[16,64,256]{2,1,0:T(8,128)(2,1)S(1)} %copy-done.6, bf16[16,64,256]{2,1,0:T(8,128)(2,1)} %collective-permute-done.20, bf16[16,64,256]{2,1,0:T(8,128)(2,1)} %collective-permute-done.19, bf16[16,64,256]{2,1,0:T(8,128)(2,1)} %collective-permute-done.18), kind=kLoop, calls=%fused_computation.3 | loop fusion | flops 2097152 | bytes 2621440 | tf_op jit(solution)/shard_map/convert_element_type | solution.py:684
  205.4 6.8 %all-to-all-start.2 = ((bf16[16,64,256]{2,1,0:T(8,128)(2,1)}), bf16[16,64,256]{2,1,0:T(8,128)(2,1)S(1)}, u32[]{:S(2)}, u32[]{:S(2)}) async-start(bf16[16,64,256]{2,1,0:T(8,128)(2,1)} %add_convert_fusion), calls=%async_computation.2 | async-start | bytes 1048576 | tf_op jit(solution)/shard_map/all_to_all | solution.py:685
  212.2 6.8 %downgrads.1 = f32[1,256,2048]{2,1,0:T(8,128)} custom-call(s32[3]{0:T(128)S(1)} %pad_add_fusion.where_ref, bf16[1280,1792]{1,0:T(8,128)(2,1)} %bitcast.8.got_rows.got_cot, bf16[640,640]{1,0:T(8,128)(2,1)} %bitcast.34, bf16[640,640]{1,0:T(8,128)(2,1)} %bitcast.29, bf16[640,640]{1,0:T(8,128)(2,1)} %copy-done.2, ...), custom_call_target="tpu_custom_call" | custom-call | flops 1500000000 | bytes 11534336 | tf_op jit(solution)/shard_map/downgrads/pallas_call | solution.py:430
  219.0 8.1 %rowgrads.1 = (f32[1,2048,256]{2,1,0:T(8,128)}, f32[1,2048,256]{2,1,0:T(8,128)}) custom-call(s32[3]{0:T(128)S(1)} %pad_add_fusion.where_ref, bf16[1280,1792]{1,0:T(8,128)(2,1)} %bitcast.8.got_rows.got_cot, bf16[640,640]{1,0:T(8,128)(2,1)} %bitcast.35, bf16[640,640]{1,0:T(8,128)(2,1)} %bitcast.30, bf16[640,640]{1,0:T(8,128)(2,1)} %copy-done.2, ...), custom_call_target="tpu_custom_call" | custom-call | flops 3000000000 | bytes 11534336 | tf_op jit(solution)/shard_map/rowgrads/pallas_call | solution.py:409
  227.1 2.9 %final.1 = bf16[512,256]{1,0:T(8,128)(2,1)} custom-call(s32[3]{0:T(128)S(1)} %pad_add_fusion.where_ref, f32[32,2,256]{2,1,0:T(2,128)S(1)} %all-to-all-done.4.pairs, f32[512,256]{1,0:T(8,128)} %get-tuple-element.56.local, f32[512,256]{1,0:T(8,128)} %get-tuple-element.57.exp, f32[512,256]{1,0:T(8,128)} %get-tuple-element.58.ca, ...), custom_call_target="tpu_custom_call" | custom-call | flops 100000000 | bytes 4194304 | tf_op jit(solution)/shard_map/final/pallas_call | solution.py:578
  230.0 0.7 convert_reduce_fusion
  (40 shorter events, 0.2 us)
Async XLA Ops:
  5.4 9.8 %copy-start.10 = (s32[512,2]{0,1:T(2,128)S(1)}, s32[512,2]{0,1:T(2,128)}, u32[]{:S(2)}) copy-start(s32[512,2]{0,1:T(2,128)} %param.17) | copy-start | bytes 12292
  5.4 10.6 %copy-start.11 = (f32[2,512]{1,0:T(2,128)S(1)}, f32[2,512]{1,0:T(2,128)}, u32[]{:S(2)}) copy-start(f32[2,512]{1,0:T(2,128)} %param.27) | copy-start | bytes 12292
  5.4 11.5 %copy-start.12 = (f32[1024]{0:T(1024)S(1)}, f32[1024]{0:T(1024)}, u32[]{:S(2)}) copy-start(f32[1024]{0:T(1024)} %param.26) | copy-start | bytes 12292
  5.4 33.3 %all-to-all-start.1 = ((bf16[32,40,640]{2,1,0:T(8,128)(2,1)}), bf16[32,40,640]{2,1,0:T(8,128)(2,1)S(1)}, u32[]{:S(2)}, u32[]{:S(2)}) async-start(bf16[32,40,640]{2,1,0:T(8,128)(2,1)} %bitcast.37), calls=%async_computation.1 | async-start | bytes 3276800 | tf_op jit(solution)/shard_map/all_to_all | solution.py:634
  38.8 5.9 %copy-start.8 = (bf16[2048,256]{1,0:T(8,128)(2,1)S(1)}, bf16[2048,256]{1,0:T(8,128)(2,1)}, u32[]{:S(2)}) copy-start(bf16[2048,256]{1,0:T(8,128)(2,1)} %whole_own.1) | copy-start | bytes 3145732
  38.8 60.8 %all-to-all-start = ((bf16[32,40,1792]{2,1,0:T(8,128)(2,1)}), bf16[32,40,1792]{2,1,0:T(8,128)(2,1)}, u32[]{:S(2)}, u32[]{:S(2)}) async-start(bf16[32,40,1792]{2,1,0:T(8,128)(2,1)} %bitcast.38), calls=%async_computation | async-start | bytes 9175040 | tf_op jit(solution)/shard_map/all_to_all | solution.py:634
  44.8 45.7 %copy-start.4 = (bf16[512,2048]{1,0:T(8,128)(2,1)S(1)}, bf16[512,2048]{1,0:T(8,128)(2,1)}, u32[]{:S(2)}) copy-start(bf16[512,2048]{1,0:T(8,128)(2,1)} %refs_1_.3) | copy-start | bytes 6291460
  44.8 45.7 %copy-start.7 = (bf16[512,256]{1,0:T(8,128)(2,1)S(1)}, bf16[512,256]{1,0:T(8,128)(2,1)}, u32[]{:S(2)}) copy-start(bf16[512,256]{1,0:T(8,128)(2,1)} %get-tuple-element.34.refs_2_) | copy-start | bytes 786436
  44.8 14.5 %collective-permute-start.6 = (bf16[1024,256]{1,0:T(8,128)(2,1)S(1)}, bf16[1024,256]{1,0:T(8,128)(2,1)S(1)}, u32[]{:S(2)}, u32[]{:S(2)}) collective-permute-start(bf16[1024,256]{1,0:T(8,128)(2,1)S(1)} %constant_dynamic-slice_fusion), channel_id=1, source_target_pairs={{0,1},{1,2},{2,3},{3,0},{4,5},{5,6},{6,7},{7,4},{8,9},{9,10},{10,1... | collective-permute-start | bytes 1572872 | tf_op jit(solution)/shard_map/ppermute | solution.py:590
  46.1 13.3 %collective-permute-start.7 = (bf16[1024,256]{1,0:T(8,128)(2,1)S(1)}, bf16[1024,256]{1,0:T(8,128)(2,1)S(1)}, u32[]{:S(2)}, u32[]{:S(2)}) collective-permute-start(bf16[1024,256]{1,0:T(8,128)(2,1)S(1)} %constant_dynamic-slice_fusion), channel_id=1, source_target_pairs={{0,3},{1,0},{2,1},{3,2},{4,7},{5,4},{6,5},{7,6},{8,11},{9,8},{10,9... | collective-permute-start | bytes 1572872 | tf_op jit(solution)/shard_map/ppermute | solution.py:590
  47.7 60.2 %copy-start = (bf16[16,40,640]{2,1,0:T(8,128)(2,1)}, bf16[16,40,640]{2,1,0:T(8,128)(2,1)S(1)}, u32[]{:S(2)}) copy-start(bf16[16,40,640]{2,1,0:T(8,128)(2,1)S(1)} %get-tuple-element.62) | copy-start | bytes 2457604
  47.7 60.2 %copy-start.1 = (bf16[16,40,640]{2,1,0:T(8,128)(2,1)}, bf16[16,40,640]{2,1,0:T(8,128)(2,1)S(1)}, u32[]{:S(2)}) copy-start(bf16[16,40,640]{2,1,0:T(8,128)(2,1)S(1)} %get-tuple-element.63) | copy-start | bytes 2457604
  47.7 40.1 %collective-permute-start = (bf16[640,640]{1,0:T(8,128)(2,1)S(1)}, bf16[640,640]{1,0:T(8,128)(2,1)S(1)}, u32[]{:S(2)}, u32[]{:S(2)}) collective-permute-start(bf16[640,640]{1,0:T(8,128)(2,1)S(1)} %bitcast.31), channel_id=1, source_target_pairs={{0,1},{1,2},{2,3},{3,0},{4,5},{5,6},{6,7},{7,4},{8,9},{9,10},{10,1... | collective-permute-start | bytes 2457608 | tf_op jit(solution)/shard_map/ppermute | solution.py:590
  47.8 40.0 %collective-permute-start.3 = (bf16[640,640]{1,0:T(8,128)(2,1)S(1)}, bf16[640,640]{1,0:T(8,128)(2,1)S(1)}, u32[]{:S(2)}, u32[]{:S(2)}) collective-permute-start(bf16[640,640]{1,0:T(8,128)(2,1)S(1)} %bitcast.26), channel_id=1, source_target_pairs={{0,3},{1,0},{2,1},{3,2},{4,7},{5,4},{6,5},{7,6},{8,11},{9,8},{10,9... | collective-permute-start | bytes 2457608 | tf_op jit(solution)/shard_map/ppermute | solution.py:590
  59.3 23.2 %collective-permute-start.8 = (bf16[512,256]{1,0:T(8,128)(2,1)S(1)}, bf16[512,256]{1,0:T(8,128)(2,1)S(1)}, u32[]{:S(2)}, u32[]{:S(2)}) collective-permute-start(bf16[512,256]{1,0:T(8,128)(2,1)S(1)} %slice.34), channel_id=1, source_target_pairs={{0,1},{1,2},{2,3},{3,0},{4,5},{5,6},{6,7},{7,4},{8,9},{9,10},{10,1... | collective-permute-start | bytes 786440 | tf_op jit(solution)/shard_map/ppermute | solution.py:590
  59.4 24.2 %collective-permute-start.9 = (bf16[512,256]{1,0:T(8,128)(2,1)S(1)}, bf16[512,256]{1,0:T(8,128)(2,1)S(1)}, u32[]{:S(2)}, u32[]{:S(2)}) collective-permute-start(bf16[512,256]{1,0:T(8,128)(2,1)S(1)} %slice.35), channel_id=1, source_target_pairs={{0,3},{1,0},{2,1},{3,2},{4,7},{5,4},{6,5},{7,6},{8,11},{9,8},{10,9... | collective-permute-start | bytes 786440 | tf_op jit(solution)/shard_map/ppermute | solution.py:590
  62.1 23.9 %collective-permute-start.10 = (bf16[1024,256]{1,0:T(8,128)(2,1)S(1)}, bf16[1024,256]{1,0:T(8,128)(2,1)S(1)}, u32[]{:S(2)}, u32[]{:S(2)}) collective-permute-start(bf16[1024,256]{1,0:T(8,128)(2,1)S(1)} %collective-permute-done.6.refs_0_), channel_id=1, source_target_pairs={{0,4},{4,0},{1,5},{5,1},{2,6},{6,2},{3,7},{7,3},{8,12},{12,8},{9,1... | collective-permute-start | bytes 1572872 | tf_op jit(solution)/shard_map/ppermute | solution.py:611
  82.4 2.3 %collective-permute-start.12 = (bf16[512,256]{1,0:T(8,128)(2,1)S(1)}, bf16[512,256]{1,0:T(8,128)(2,1)S(1)}, u32[]{:S(2)}, u32[]{:S(2)}) collective-permute-start(bf16[512,256]{1,0:T(8,128)(2,1)S(1)} %collective-permute-done.8.refs_2_), channel_id=1, source_target_pairs={{0,4},{4,0},{1,5},{5,1},{2,6},{6,2},{3,7},{7,3},{8,12},{12,8},{9,1... | collective-permute-start | bytes 786440 | tf_op jit(solution)/shard_map/ppermute | solution.py:611
  83.6 1.5 collective-permute-start.13
  84.7 8.0 %collective-permute-start.11 = (bf16[1024,256]{1,0:T(8,128)(2,1)S(1)}, bf16[1024,256]{1,0:T(8,128)(2,1)S(1)}, u32[]{:S(2)}, u32[]{:S(2)}) collective-permute-start(bf16[1024,256]{1,0:T(8,128)(2,1)S(1)} %collective-permute-done.7.refs_1_), channel_id=1, source_target_pairs={{0,4},{4,0},{1,5},{5,1},{2,6},{6,2},{3,7},{7,3},{8,12},{12,8},{9,1... | collective-permute-start | bytes 1572872 | tf_op jit(solution)/shard_map/ppermute | solution.py:611
  85.1 20.7 %collective-permute-start.1 = (bf16[640,640]{1,0:T(8,128)(2,1)S(1)}, bf16[640,640]{1,0:T(8,128)(2,1)}, u32[]{:S(2)}, u32[]{:S(2)}) collective-permute-start(bf16[640,640]{1,0:T(8,128)(2,1)S(1)} %bitcast.27), channel_id=1, source_target_pairs={{0,1},{1,2},{2,3},{3,0},{4,5},{5,6},{6,7},{7,4},{8,9},{9,10},{10,1... | collective-permute-start | bytes 2457608 | tf_op jit(solution)/shard_map/ppermute | solution.py:590
  86.0 21.0 %collective-permute-start.2 = (bf16[640,640]{1,0:T(8,128)(2,1)S(1)}, bf16[640,640]{1,0:T(8,128)(2,1)}, u32[]{:S(2)}, u32[]{:S(2)}) collective-permute-start(bf16[640,640]{1,0:T(8,128)(2,1)S(1)} %bitcast.32), channel_id=1, source_target_pairs={{0,3},{1,0},{2,1},{3,2},{4,7},{5,4},{6,5},{7,6},{8,11},{9,8},{10,9... | collective-permute-start | bytes 2457608 | tf_op jit(solution)/shard_map/ppermute | solution.py:590
  87.8 20.1 %copy-start.2 = (bf16[640,640]{1,0:T(8,128)(2,1)}, bf16[640,640]{1,0:T(8,128)(2,1)S(1)}, u32[]{:S(2)}) copy-start(bf16[640,640]{1,0:T(8,128)(2,1)S(1)} %collective-permute-done.refs_2_) | copy-start | bytes 2457604
  87.8 35.6 %collective-permute-start.4 = (bf16[640,640]{1,0:T(8,128)(2,1)S(1)}, bf16[640,640]{1,0:T(8,128)(2,1)}, u32[]{:S(2)}, u32[]{:S(2)}) collective-permute-start(bf16[640,640]{1,0:T(8,128)(2,1)S(1)} %collective-permute-done.refs_2_), channel_id=1, source_target_pairs={{0,1},{1,2},{2,3},{3,0},{4,5},{5,6},{6,7},{7,4},{8,9},{9,10},{10,1... | collective-permute-start | bytes 2457608 | tf_op jit(solution)/shard_map/ppermute | solution.py:590
  87.8 20.1 %copy-start.3 = (bf16[640,640]{1,0:T(8,128)(2,1)}, bf16[640,640]{1,0:T(8,128)(2,1)S(1)}, u32[]{:S(2)}) copy-start(bf16[640,640]{1,0:T(8,128)(2,1)S(1)} %collective-permute-done.3.refs_5_) | copy-start | bytes 2457604
  87.8 35.6 %collective-permute-start.5 = (bf16[640,640]{1,0:T(8,128)(2,1)S(1)}, bf16[640,640]{1,0:T(8,128)(2,1)}, u32[]{:S(2)}, u32[]{:S(2)}) collective-permute-start(bf16[640,640]{1,0:T(8,128)(2,1)S(1)} %collective-permute-done.3.refs_5_), channel_id=1, source_target_pairs={{0,3},{1,0},{2,1},{3,2},{4,7},{5,4},{6,5},{7,6},{8,11},{9,8},{10,9... | collective-permute-start | bytes 2457608 | tf_op jit(solution)/shard_map/ppermute | solution.py:590
  101.5 43.4 %collective-permute-start.14 = (bf16[1280,256]{1,0:T(8,128)(2,1)}, bf16[1280,256]{1,0:T(8,128)(2,1)}, u32[]{:S(2)}, u32[]{:S(2)}) collective-permute-start(bf16[1280,256]{1,0:T(8,128)(2,1)} %slice.36.refs_0_), channel_id=1, source_target_pairs={{0,1},{1,2},{2,3},{3,0},{4,5},{5,6},{6,7},{7,4},{8,9},{9,10},{10,1... | collective-permute-start | bytes 1966088 | tf_op jit(solution)/shard_map/ppermute | solution.py:590
  105.9 39.0 %collective-permute-start.15 = (bf16[1280,256]{1,0:T(8,128)(2,1)}, bf16[1280,256]{1,0:T(8,128)(2,1)}, u32[]{:S(2)}, u32[]{:S(2)}) collective-permute-start(bf16[1280,256]{1,0:T(8,128)(2,1)} %slice.36.refs_0_), channel_id=1, source_target_pairs={{0,3},{1,0},{2,1},{3,2},{4,7},{5,4},{6,5},{7,6},{8,11},{9,8},{10,9... | collective-permute-start | bytes 1966088 | tf_op jit(solution)/shard_map/ppermute | solution.py:590
  107.0 45.4 %collective-permute-start.16 = (bf16[1280,256]{1,0:T(8,128)(2,1)}, bf16[1280,256]{1,0:T(8,128)(2,1)}, u32[]{:S(2)}, u32[]{:S(2)}) collective-permute-start(bf16[1280,256]{1,0:T(8,128)(2,1)} %slice.36.refs_0_), channel_id=1, source_target_pairs={{0,2},{1,3},{2,0},{3,1},{4,6},{5,7},{6,4},{7,5},{8,10},{9,11},{10,... | collective-permute-start | bytes 1966088 | tf_op jit(solution)/shard_map/ppermute | solution.py:590
  133.6 52.1 %all-to-all-start.3 = ((bf16[128,40,256]{2,1,0:T(8,128)(2,1)}), bf16[128,40,256]{2,1,0:T(8,128)(2,1)S(1)}, u32[]{:S(2)}, u32[]{:S(2)}) async-start(bf16[128,40,256]{2,1,0:T(8,128)(2,1)} %bitcast.39), calls=%async_computation.3 | async-start | bytes 5242880 | tf_op jit(solution)/shard_map/all_to_all | solution.py:672
  163.4 13.5 %copy-start.5 = (bf16[512,2048]{1,0:T(8,128)(2,1)S(1)}, bf16[512,2048]{1,0:T(8,128)(2,1)}, u32[]{:S(2)}) copy-start(bf16[512,2048]{1,0:T(8,128)(2,1)} %refs_1_.3) | copy-start | bytes 6291460
  163.4 13.5 %copy-start.9 = (bf16[2048,256]{1,0:T(8,128)(2,1)S(1)}, bf16[2048,256]{1,0:T(8,128)(2,1)}, u32[]{:S(2)}) copy-start(bf16[2048,256]{1,0:T(8,128)(2,1)} %whole_own.1) | copy-start | bytes 3145732
  163.4 6.1 %collective-permute-start.17 = (bf16[4,16,64,256]{3,2,1,0:T(8,128)(2,1)S(1)}, bf16[4,16,64,256]{3,2,1,0:T(8,128)(2,1)S(1)}, u32[]{:S(2)}, u32[]{:S(2)}) collective-permute-start(bf16[4,16,64,256]{3,2,1,0:T(8,128)(2,1)S(1)} %slice_bitcast_fusion), channel_id=1, source_target_pairs={{0,4},{4,0},{1,5},{5,1},{2,6},{6,2},{3,7},{7,3},{8,12},{12,8},{9,1... | collective-permute-start | bytes 6291464 | tf_op jit(solution)/shard_map/ppermute | solution.py:681
  172.6 22.7 %collective-permute-start.18 = (bf16[16,64,256]{2,1,0:T(8,128)(2,1)}, bf16[16,64,256]{2,1,0:T(8,128)(2,1)}, u32[]{:S(2)}, u32[]{:S(2)}) collective-permute-start(bf16[16,64,256]{2,1,0:T(8,128)(2,1)} %get-tuple-element.44), channel_id=1, source_target_pairs={{0,1},{1,2},{2,3},{3,0},{4,5},{5,6},{6,7},{7,4},{8,9},{9,10},{10,1... | collective-permute-start | bytes 1572872 | tf_op jit(solution)/shard_map/ppermute | solution.py:590
  173.8 21.5 %collective-permute-start.19 = (bf16[16,64,256]{2,1,0:T(8,128)(2,1)}, bf16[16,64,256]{2,1,0:T(8,128)(2,1)}, u32[]{:S(2)}, u32[]{:S(2)}) collective-permute-start(bf16[16,64,256]{2,1,0:T(8,128)(2,1)} %get-tuple-element.45), channel_id=1, source_target_pairs={{0,3},{1,0},{2,1},{3,2},{4,7},{5,4},{6,5},{7,6},{8,11},{9,8},{10,9... | collective-permute-start | bytes 1572872 | tf_op jit(solution)/shard_map/ppermute | solution.py:590
  175.7 27.2 %collective-permute-start.20 = (bf16[16,64,256]{2,1,0:T(8,128)(2,1)}, bf16[16,64,256]{2,1,0:T(8,128)(2,1)}, u32[]{:S(2)}, u32[]{:S(2)}) collective-permute-start(bf16[16,64,256]{2,1,0:T(8,128)(2,1)} %get-tuple-element.46), channel_id=1, source_target_pairs={{0,2},{1,3},{2,0},{3,1},{4,6},{5,7},{6,4},{7,5},{8,10},{9,11},{10,... | collective-permute-start | bytes 1572872 | tf_op jit(solution)/shard_map/ppermute | solution.py:590
  185.7 17.2 %copy-start.6 = (bf16[16,64,256]{2,1,0:T(8,128)(2,1)S(1)}, bf16[16,64,256]{2,1,0:T(8,128)(2,1)}, u32[]{:S(2)}) copy-start(bf16[16,64,256]{2,1,0:T(8,128)(2,1)} %get-tuple-element.47) | copy-start | bytes 1572868
  190.3 15.1 %all-to-all-start.4 = ((f32[32,2,256]{2,1,0:T(2,128)}), f32[32,2,256]{2,1,0:T(2,128)S(1)}, u32[]{:S(2)}, u32[]{:S(2)}) async-start(f32[32,2,256]{2,1,0:T(2,128)} %get-tuple-element.55), calls=%async_computation.4 | async-start | bytes 131072 | tf_op jit(solution)/shard_map/all_to_all | solution.py:690
  205.4 24.6 %all-to-all-start.2 = ((bf16[16,64,256]{2,1,0:T(8,128)(2,1)}), bf16[16,64,256]{2,1,0:T(8,128)(2,1)S(1)}, u32[]{:S(2)}, u32[]{:S(2)}) async-start(bf16[16,64,256]{2,1,0:T(8,128)(2,1)} %add_convert_fusion), calls=%async_computation.2 | async-start | bytes 1048576 | tf_op jit(solution)/shard_map/all_to_all | solution.py:685
